TPU v7x, 32 devices: a whole 2x2x4 slice. The times are simulated.
32 devices in a mesh: sp: 4 (over z), fs: 4 (over y, x), tp: 2 (over core).
Axes of the slice: x: 2, y: 2, z: 4, core: 2. Of those that a mesh axis runs over, the one named last changes fastest.
Arguments:
- stream: bfloat16 [4, 1024, 2048], P('fs', 'sp'), may hold values from -6 to 6
- norm_gain: bfloat16 [2048], replicated, may hold values from 0.099609375 to 1.8984375
- query_weight: bfloat16 [2048, 1024], P(None, 'tp'), may hold values from -0.125 to 0.125
- key_weight: bfloat16 [2048, 1024], P(None, 'tp'), may hold values from -0.125 to 0.125
- value_weight: bfloat16 [2048, 1024], P(None, 'tp'), may hold values from -0.125 to 0.125
- filter_input: bfloat16 [2048, 1024], P(None, 'tp'), may hold values from -0.125 to 0.125
- filter_gate: bfloat16 [2048, 1024], P(None, 'tp'), may hold values from -0.125 to 0.125
- score_offset: bfloat16 [4, 1024, 16], P('fs', 'sp', 'tp'), may hold values from -16 to 0
- head_gain: bfloat16 [1024], P('tp'), may hold values from 0.099609375 to 1.8984375
- filter_taps: bfloat16 [31, 1024], P(None, 'tp'), may hold values from -5 to 5
- channel_gain: bfloat16 [1024], P('tp'), may hold values from 0.099609375 to 1.8984375
- channel_shift: bfloat16 [1024], P('tp'), may hold values from -3 to 3
- attend_out: bfloat16 [1024, 2048], P('tp'), may hold values from -0.125 to 0.125
- filter_out: bfloat16 [1024, 2048], P('tp'), may hold values from -0.125 to 0.125
Outputs:
- mixed_out: bfloat16 [4, 1024, 2048], P('fs', ('sp', 'tp'))
- mass_log: float32 [4, 1024, 16], P('fs', 'sp', 'tp')
All inputs are finite; a program needn't handle non-finite values.
Results may differ from a plain program's by a relative error of at most 0.015.
Values may be sent and summed in bfloat16 or wider, within the bound.
A program may use at most 64 MiB of HBM per device.

v0:
```python
import functools

import jax
import jax.numpy as jnp
from jax import lax
from jax.experimental import pallas as pl
from jax.experimental.pallas import tpu as pltpu
from jax.sharding import PartitionSpec as P

HEAD_DIM = 64

rms_eps = 1e-06
norm_eps = 1e-05
mass_floor = 0.01
HALO = 32
MESH = pl.DeviceIdType.MESH


def kernel(
    n, tp, taps, hp, total_channels,
    stream_hbm, ngain, offs, raw_taps, gain_ref, cgain_ref, cshift_ref,
    q_hbm, k_hbm, v_hbm, in_hbm, gate_hbm, attend_hbm, filter_hbm,
    out_ref, log_ref,
    stream, stream_sem, mass_ref, arrived_ref, tap_ref, gains, normed, weights, out_weights, packet, got, offs_got, heads_ref, conv_ref, conv_share, leaving,
    piece, home, mass_piece, gated, halo, ext, filt, stats, stats_got,
    weight_sem, out_weight_sem, offs_send, offs_recv, out_send, out_recv,
    send_sem, recv_sem, back_send, back_recv, mass_send, mass_recv,
    halo_send, halo_recv, stat_send, stat_recv,
):
    f32, bf16 = jnp.float32, jnp.bfloat16
    me = lax.axis_index("sp")
    core = lax.axis_index("tp")
    rows = normed.shape[0]
    chans = in_hbm.shape[1]
    lanes = hp * HEAD_DIM

    fetches = [
        pltpu.make_async_copy(w, weights.at[t], weight_sem.at[t])
        for t, w in enumerate((q_hbm, k_hbm, v_hbm, in_hbm, gate_hbm))
    ]
    fetches += [
        pltpu.make_async_copy(w, out_weights.at[t], out_weight_sem.at[t])
        for t, w in enumerate((filter_hbm, attend_hbm))
    ]
    first = pltpu.make_async_copy(stream_hbm, stream, stream_sem)
    first.start()
    fetches[0].start()
    fetches[1].start()

    barrier = pltpu.get_barrier_semaphore()
    for r in range(1, n):
        pl.semaphore_signal(barrier, inc=1, device_id={"sp": lax.rem(me + r, n)}, device_id_type=MESH)
    for r in range(1, tp):
        pl.semaphore_signal(barrier, inc=1, device_id={"tp": lax.rem(core + r, tp)}, device_id_type=MESH)

    tap_ref[:taps] = raw_taps[...].astype(f32)
    for j in range(n):
        gains[j] = gain_ref[j * lanes:(j + 1) * lanes].astype(f32).reshape(1, lanes)
    norm_gain = ngain[...].astype(f32).reshape(1, -1)
    band = min(64, rows)

    first.wait()

    @pl.loop(0, rows // band)
    def _(c):
        some = pl.ds(pl.multiple_of(c * band, band), band)
        x = stream[some, :].astype(f32)
        x = x * lax.rsqrt(jnp.mean(x * x, axis=-1, keepdims=True) + rms_eps)
        normed[some, :] = (x * norm_gain).astype(bf16)

    pl.semaphore_wait(barrier, n - 1 + tp - 1)
    sends = []
    for r in range(1, n):
        to = lax.rem(me + r, n)
        copy = pltpu.make_async_remote_copy(
            src_ref=offs, dst_ref=offs_got.at[me], send_sem=offs_send.at[r],
            recv_sem=offs_recv.at[me], device_id={"sp": to}, device_id_type=MESH)
        copy.start()
        sends.append(copy)
    offs_got[me] = offs[...]
    group = max(1, 256 // lanes)
    for t in range(3):
        fetches[t].wait()
        fetches[t + 2].start()
        for j in range(0, n, group):
            wide = min(group, n - j) * lanes
            y = jnp.dot(normed[...], weights[t, :, j * lanes:j * lanes + wide], preferred_element_type=f32)
            y = y.astype(bf16)
            if t == 0:
                y = y * jnp.asarray(HEAD_DIM ** (-0.5), bf16)
            for u in range(wide // lanes):
                packet[t, j + u] = y[:, u * lanes:(u + 1) * lanes]
        for r in range(1, n):
            to = lax.rem(me + r, n)
            copy = pltpu.make_async_remote_copy(
                src_ref=packet.at[t, to], dst_ref=got.at[t, me], send_sem=send_sem.at[t, r],
                recv_sem=recv_sem.at[t, me], device_id={"sp": to}, device_id_type=MESH)
            copy.start()
            sends.append(copy)
        got[t, me] = packet[t, me]

    width = min(256, chans)
    fetches[3].wait()
    fetches[4].wait()
    fetches[5].start()
    fetches[6].start()

    @pl.loop(0, chans // width)
    def _(c):
        cols = pl.ds(pl.multiple_of(c * width, width), width)
        x = normed[...]
        value = jnp.dot(x, weights[3, :, cols], preferred_element_type=f32).astype(bf16).astype(f32)
        gate = jnp.dot(x, weights[4, :, cols], preferred_element_type=f32).astype(bf16).astype(f32)
        g = (value * jax.nn.sigmoid(gate)).astype(bf16)
        gated[:, cols] = g[rows - HALO:]
        ext[HALO:, cols] = g.astype(f32)

    halo_copy = pltpu.make_async_remote_copy(
        src_ref=gated, dst_ref=halo, send_sem=halo_send, recv_sem=halo_recv,
        device_id={"sp": lax.rem(me + 1, n)}, device_id_type=MESH)
    halo_copy.start()
    step = min(128, rows)

    def convolve(starts):
        @pl.loop(0, chans // 128)
        def _(c):
            cols = pl.ds(pl.multiple_of(c * 128, 128), 128)
            for r0 in starts:
                acc = jnp.zeros((step, 128), f32)
                for k in range(taps):
                    start = HALO - (taps - 1) + k + r0
                    acc = acc + ext[start:start + step, cols] * tap_ref[k:k + 1, cols]
                filt[r0:r0 + step, cols] = acc

    stat_copies = []

    def finish_rows():
        halo_copy.wait()
        ext[:HALO, :] = jnp.where(me > 0, halo[...].astype(f32), 0.0)
        convolve([0])
        f = filt[...]
        lsum = jnp.sum(f, axis=1, keepdims=True)
        dev = f - lsum * (1.0 / chans)
        lsq = jnp.sum(dev * dev, axis=1, keepdims=True)
        lane_s = lax.broadcasted_iota(jnp.int32, (rows, 128), 1)
        stats[...] = jnp.where(lane_s < 64, lsum, lsq)
        for r in range(1, tp):
            to = lax.rem(core + r, tp)
            copy = pltpu.make_async_remote_copy(
                src_ref=stats, dst_ref=stats_got.at[core], send_sem=stat_send.at[r],
                recv_sem=stat_recv.at[core], device_id={"tp": to}, device_id_type=MESH)
            copy.start()
            stat_copies.append(copy)

    convolve(range(step, rows, step))

    ri = lax.broadcasted_iota(jnp.int32, (rows, rows), 0)
    ci = lax.broadcasted_iota(jnp.int32, (rows, rows), 1)
    strict = ci < ri
    tri = (ri >= ci).astype(bf16)
    lane = lax.broadcasted_iota(jnp.int32, (rows, lanes), 1)
    gain = gains[me]
    head_row = lax.broadcasted_iota(jnp.int32, (offs.shape[0], rows), 0)
    waited = set()
    for i in [*range(n - 2), n - 1, n - 2]:
        if i == n - 1:
            finish_rows()

        for j in range(i + 1):
            if j in waited:
                continue
            waited.add(j)

            @pl.when(me != j)
            def _(j=j):
                pltpu.make_async_remote_copy(
                    src_ref=offs, dst_ref=offs_got.at[j], send_sem=offs_send.at[0],
                    recv_sem=offs_recv.at[j], device_id={"sp": j}, device_id_type=MESH).wait_recv()
                for t in range(3):
                    pltpu.make_async_remote_copy(
                        src_ref=packet.at[t, j], dst_ref=got.at[t, j], send_sem=send_sem.at[t, 0],
                        recv_sem=recv_sem.at[t, j], device_id={"sp": j}, device_id_type=MESH).wait_recv()

        q = got[0, i]
        result = jnp.zeros((rows, lanes), f32)
        masses = jnp.zeros((rows, 128), f32)
        lane_m = lax.broadcasted_iota(jnp.int32, (rows, 128), 1)
        for h in range(hp):
            mine = (lane >= h * HEAD_DIM) & (lane < (h + 1) * HEAD_DIM)
            qh = jnp.where(mine, q, jnp.zeros_like(q))
            acc = jnp.zeros((rows, lanes), f32)
            mass = jnp.zeros((rows, 1), f32)
            carry = jnp.zeros((rows, 1), f32)
            for kb in range(i, -1, -1):
                kk = got[1, kb]
                vv = got[2, kb]
                off = jnp.sum(jnp.where(head_row == me * hp + h, offs_got[kb].astype(f32), 0.0),
                              axis=0, keepdims=True)
                z = lax.dot_general(qh, kk, (((1,), (1,)), ((), ())), preferred_element_type=f32) + off
                lose = -(jnp.maximum(z, 0.0) + jnp.log(1.0 + jnp.exp(-jnp.abs(z))))
                if kb == i:
                    lose = jnp.where(strict, lose, 0.0)
                hi = lose.astype(bf16)
                lo = (lose - hi.astype(f32)).astype(bf16)
                cum = (jnp.dot(hi, tri, preferred_element_type=f32)
                       + jnp.dot(lo, tri, preferred_element_type=f32))
                w = jnp.exp(z + cum + carry)
                if kb == i:
                    w = jnp.where(strict, w, 0.0)
                mass = mass + jnp.sum(w, axis=1, keepdims=True)
                acc = acc + jnp.dot(w.astype(bf16), vv, preferred_element_type=f32)
                carry = carry + cum[:, 0:1]
            sq = jnp.sum(jnp.where(mine, acc * acc, 0.0), axis=1, keepdims=True)
            scaled = acc * lax.rsqrt(sq * (1.0 / HEAD_DIM) + rms_eps)
            result = jnp.where(mine, scaled, result)
            masses = jnp.where(lane_m == h, mass, masses)
        piece[i] = (result * gain).astype(bf16)
        mass_piece[i] = jnp.transpose(masses)[:8]

        @pl.when(me != i)
        def _():
            pltpu.make_async_remote_copy(
                src_ref=piece.at[i], dst_ref=home.at[me], send_sem=back_send.at[i],
                recv_sem=back_recv.at[me], device_id={"sp": i}, device_id_type=MESH).start()
            pltpu.make_async_remote_copy(
                src_ref=mass_piece.at[i], dst_ref=mass_ref.at[me], send_sem=mass_send.at[i],
                recv_sem=mass_recv.at[me], device_id={"sp": i}, device_id_type=MESH).start()

    mean = stats[:, 0:1]
    for r in range(1, tp):
        frm = lax.rem(core + r, tp)
        pltpu.make_async_remote_copy(
            src_ref=stats, dst_ref=stats_got.at[frm], send_sem=stat_send.at[0],
            recv_sem=stat_recv.at[frm], device_id={"tp": frm}, device_id_type=MESH).wait_recv()
        mean = mean + stats_got[frm][:, 0:1]
    mean = mean * (1.0 / total_channels)
    apart = stats[:, 0:1] * (1.0 / chans) - mean
    spread = stats[:, 64:65] + chans * apart * apart
    for r in range(1, tp):
        frm = lax.rem(core + r, tp)
        other = stats_got[frm]
        apart = other[:, 0:1] * (1.0 / chans) - mean
        spread = spread + other[:, 64:65] + chans * apart * apart
    scale = lax.rsqrt(spread * (1.0 / total_channels) + norm_eps)
    y = (filt[...] - mean) * scale * cgain_ref[...].astype(f32).reshape(1, -1) + cshift_ref[...].astype(f32).reshape(1, -1)
    conv_ref[...] = (y * jax.nn.sigmoid(y)).astype(bf16)

    fetches[5].wait()
    fetches[6].wait()
    model = out_weights.shape[2]
    tile = min(512, model)
    for c in range(0, model, tile):
        conv_share[:, c:c + tile] = jnp.dot(
            conv_ref[...], out_weights[0, :, c:c + tile], preferred_element_type=f32)

    for j in range(n):
        @pl.when(me != j)
        def _():
            pltpu.make_async_remote_copy(
                src_ref=piece.at[j], dst_ref=home.at[j], send_sem=back_send.at[j],
                recv_sem=back_recv.at[j], device_id={"sp": j}, device_id_type=MESH).wait()
            pltpu.make_async_remote_copy(
                src_ref=mass_piece.at[j], dst_ref=mass_ref.at[j], send_sem=mass_send.at[j],
                recv_sem=mass_recv.at[j], device_id={"sp": j}, device_id_type=MESH).wait()
            heads_ref[:, j * lanes:(j + 1) * lanes] = home[j]

        @pl.when(me == j)
        def _():
            heads_ref[:, j * lanes:(j + 1) * lanes] = piece[j]
            mass_ref[j] = mass_piece[j]
    share = rows // tp
    partner = 1 - core
    theirs = pl.ds(pl.multiple_of(partner * share, share), share)
    ours = pl.ds(pl.multiple_of(core * share, share), share)
    leaves = []
    for c in range(0, model, tile):
        cols = slice(c, c + tile)
        leaving[:, cols] = (conv_share[theirs, cols] + jnp.dot(
            heads_ref[theirs, :], out_weights[1, :, cols], preferred_element_type=f32)).astype(bf16)
        copy = pltpu.make_async_remote_copy(
            src_ref=leaving.at[:, pl.ds(c, tile)], dst_ref=arrived_ref.at[:, pl.ds(c, tile)],
            send_sem=out_send.at[c // tile], recv_sem=out_recv.at[c // tile],
            device_id={"tp": partner}, device_id_type=MESH)
        copy.start()
        leaves.append(copy)
    for j in range(n):
        log_ref[j * hp:(j + 1) * hp] = jnp.log(jnp.maximum(mass_ref[j][:hp], mass_floor))
    for c in range(0, model, tile):
        cols = slice(c, c + tile)
        mine = conv_share[ours, cols] + jnp.dot(
            heads_ref[ours, :], out_weights[1, :, cols], preferred_element_type=f32)
        leaves[c // tile].wait()
        out_ref[:, cols] = (mine + arrived_ref[:, cols].astype(f32)).astype(bf16)
    for copy in sends + stat_copies:
        copy.wait_send()


def place(mixed, mass_log, out_ref, log_ref, sem):
    copies = [
        pltpu.make_async_copy(mixed, out_ref, sem.at[0]),
        pltpu.make_async_copy(mass_log, log_ref, sem.at[1]),
    ]
    for copy in copies:
        copy.start()
    for copy in copies:
        copy.wait()


def local(n, tp,
    stream, norm_gain, query_weight, key_weight, value_weight, filter_input, filter_gate,
    score_offset, head_gain, filter_taps, channel_gain, channel_shift, attend_out, filter_out,
):
    f32, bf16 = jnp.float32, jnp.bfloat16
    rows = stream.shape[1]
    heads = score_offset.shape[2]
    hp = heads // n
    lanes = hp * HEAD_DIM
    chans = filter_input.shape[1]
    taps = filter_taps.shape[0]
    model = stream.shape[2]
    share = rows // tp
    tiles = model // min(512, model)

    vmem = pl.BlockSpec(memory_space=pltpu.VMEM)
    hbm = pl.BlockSpec(memory_space=pl.ANY)
    dma = pltpu.SemaphoreType.DMA
    mixed, mass_log = pl.pallas_call(
        functools.partial(kernel, n, tp, taps, hp, chans * tp),
        out_shape=(
            jax.ShapeDtypeStruct((share, model), bf16),
            jax.ShapeDtypeStruct((heads, rows), f32),
        ),
        in_specs=[hbm] + [vmem] * 6 + [hbm] * 7,
        out_specs=(vmem,) * 2,
        scratch_shapes=[
            pltpu.VMEM((rows, model), bf16),
            dma,
            pltpu.VMEM((n, 8, rows), f32),
            pltpu.VMEM((share, model), bf16),
            pltpu.VMEM((taps + -taps % 8, chans), f32),
            pltpu.VMEM((n, 1, lanes), f32),
            pltpu.VMEM((rows, model), bf16),
            pltpu.VMEM((5, model, chans), bf16),
            pltpu.VMEM((2, chans, model), bf16),
            pltpu.VMEM((3, n, rows, lanes), bf16),
            pltpu.VMEM((3, n, rows, lanes), bf16),
            pltpu.VMEM((n, heads, rows), bf16),
            pltpu.VMEM((rows, heads * HEAD_DIM), bf16),
            pltpu.VMEM((rows, chans), bf16),
            pltpu.VMEM((rows, model), f32),
            pltpu.VMEM((share, model), bf16),
            pltpu.VMEM((n, rows, lanes), bf16),
            pltpu.VMEM((n, rows, lanes), bf16),
            pltpu.VMEM((n, 8, rows), f32),
            pltpu.VMEM((HALO, chans), bf16),
            pltpu.VMEM((HALO, chans), bf16),
            pltpu.VMEM((HALO + rows, chans), f32),
            pltpu.VMEM((rows, chans), f32),
            pltpu.VMEM((rows, 128), f32),
            pltpu.VMEM((tp, rows, 128), f32),
            dma((5,)), dma((2,)), dma((n,)), dma((n,)), dma((tiles,)), dma((tiles,)),
            dma((3, n)), dma((3, n)), dma((n,)), dma((n,)), dma((n,)), dma((n,)),
            dma, dma, dma((tp,)), dma((tp,)),
        ],
        compiler_params=pltpu.CompilerParams(
            collective_id=0, has_side_effects=True, vmem_limit_bytes=56 * 1024 * 1024),
    )(stream[0], norm_gain, score_offset[0].T, filter_taps, head_gain, channel_gain, channel_shift,
      query_weight, key_weight, value_weight, filter_input, filter_gate, attend_out, filter_out)
    mixed, mass_log = pl.pallas_call(
        place,
        out_shape=(
            jax.ShapeDtypeStruct((share, model), bf16),
            jax.ShapeDtypeStruct((heads, rows), f32),
        ),
        in_specs=[vmem] * 2,
        out_specs=(hbm,) * 2,
        scratch_shapes=[dma((2,))],
    )(mixed, mass_log)
    return (mixed[None], mass_log.T[None])


def shifted(value, axis, steps):
    count = lax.axis_size(axis)
    first, last = (max(0, -steps), min(count, count - steps))
    return lax.ppermute(value, axis, [(source, source + steps) for source in range(first, last)])


def local_ring(
    stream,
    norm_gain,
    query_weight,
    key_weight,
    value_weight,
    filter_input,
    filter_gate,
    score_offset,
    head_gain,
    filter_taps,
    channel_gain,
    channel_shift,
    attend_out,
    filter_out,
):
    rows_here = stream.shape[1]
    total_channels = filter_input.shape[1] * lax.axis_size("tp")
    xfloat = stream[0].astype(jnp.float32)
    normed = xfloat * lax.rsqrt(jnp.mean(xfloat * xfloat, axis=-1, keepdims=True) + rms_eps)
    normed = (normed * norm_gain.astype(jnp.float32)).astype(jnp.bfloat16)

    def project(weight):
        return jnp.dot(normed, weight, preferred_element_type=jnp.float32).astype(jnp.bfloat16)

    queries = project(query_weight)
    keys_here = project(key_weight)
    values_here = project(value_weight)
    conv_in = project(filter_input)
    conv_gate = project(filter_gate)
    offsets_here = score_offset[0]
    heads_here = offsets_here.shape[1]
    first_pos = lax.axis_index("sp") * rows_here
    position = first_pos + jnp.arange(rows_here, dtype=jnp.int32)
    qheads = queries.reshape(rows_here, heads_here, HEAD_DIM)

    def absorb(state_now, kblock, vblock, oblock, first_key):
        attended, weight_mass, survive = state_now
        span = kblock.shape[0]
        kblock = kblock.reshape(span, heads_here, HEAD_DIM)
        vblock = vblock.reshape(span, heads_here, HEAD_DIM)
        scores = jnp.einsum(
            "thd,shd->hts", qheads, kblock, preferred_element_type=jnp.float32
        ) * HEAD_DIM ** (-0.5)
        scores = scores + oblock.astype(jnp.float32).T[:, None, :]
        key_pos = first_key + jnp.arange(span, dtype=jnp.int32)
        strict = ((key_pos[None, :] < position[:, None]) & (key_pos[None, :] >= 0))[None]
        losing = jnp.where(strict, jax.nn.log_sigmoid(-scores), 0.0)
        beyond = lax.cumsum(losing, axis=2, reverse=True) - losing + survive[:, :, None]
        weights = jnp.where(strict, jnp.exp(jax.nn.log_sigmoid(scores) + beyond), 0.0)
        weight_mass = weight_mass + jnp.sum(weights, axis=2)
        attended = attended + jnp.einsum(
            "hts,shd->thd", weights.astype(jnp.bfloat16), vblock, preferred_element_type=jnp.float32
        )
        survive = survive + jnp.sum(losing, axis=2)
        return (attended, weight_mass, survive)

    initial = (
        jnp.zeros((rows_here, heads_here, HEAD_DIM), jnp.float32),
        jnp.zeros((heads_here, rows_here), jnp.float32),
        jnp.zeros((heads_here, rows_here), jnp.float32),
    )
    state_now = absorb(initial, keys_here, values_here, offsets_here, first_pos)

    def pass_turn(turn_index, carried):
        state_now, travelling = carried
        travelling = shifted((travelling[0], travelling[1], travelling[2]), "sp", 1)
        first_key = first_pos - (turn_index + 1) * rows_here
        state_now = absorb(state_now, travelling[0], travelling[1], travelling[2], first_key)
        return (state_now, travelling)

    state_now, travelling = lax.fori_loop(
        0, lax.axis_size("sp") - 1, pass_turn, (state_now, (keys_here, values_here, offsets_here))
    )
    attended, weight_mass, survive = state_now
    head_scale = lax.rsqrt(jnp.mean(attended * attended, axis=-1, keepdims=True) + rms_eps)
    heads_flat = attended * head_scale * head_gain.astype(jnp.float32).reshape(heads_here, HEAD_DIM)
    heads_flat = heads_flat.astype(jnp.bfloat16).reshape(rows_here, heads_here * HEAD_DIM)
    mass_log = jnp.log(jnp.maximum(weight_mass.T, mass_floor))
    gated_rows = (
        conv_in.astype(jnp.float32) * jax.nn.sigmoid(conv_gate.astype(jnp.float32))
    ).astype(jnp.bfloat16)
    reach_back = filter_taps.shape[0] - 1
    earlier = shifted(gated_rows[rows_here - reach_back :], "sp", 1)
    extended = jnp.concatenate([earlier, gated_rows], axis=0).astype(jnp.float32)
    tap_values = filter_taps.astype(jnp.float32)
    filtered = jnp.zeros((rows_here, gated_rows.shape[1]), jnp.float32)
    for tap_index in range(reach_back + 1):
        filtered = filtered + extended[tap_index : tap_index + rows_here] * tap_values[tap_index]
    center = lax.psum(jnp.sum(filtered, axis=-1), "tp") / total_channels
    deviation = filtered - center[:, None]
    spread = lax.psum(jnp.sum(deviation * deviation, axis=-1), "tp") / total_channels
    conv_out = jax.nn.silu(
        deviation * lax.rsqrt(spread[:, None] + norm_eps) * channel_gain.astype(jnp.float32)
        + channel_shift.astype(jnp.float32)
    ).astype(jnp.bfloat16)
    mixed_out = lax.psum_scatter(
        (
            jnp.dot(heads_flat, attend_out, preferred_element_type=jnp.float32)
            + jnp.dot(conv_out, filter_out, preferred_element_type=jnp.float32)
        ).astype(jnp.bfloat16),
        "tp",
        scatter_dimension=0,
        tiled=True,
    )
    return (mixed_out[None], mass_log[None])


def solution(mesh):
    n, tp = mesh.shape["sp"], mesh.shape["tp"]

    def choose(*args):
        heads = args[7].shape[2]
        if tp == 2 and n > 1 and heads % n == 0 and (heads // n * HEAD_DIM) % 128 == 0:
            return local(n, tp, *args)
        return local_ring(*args)

    return jax.shard_map(
        choose,
        mesh=mesh,
        in_specs=(
            P("fs", "sp", None), P(), P(None, "tp"), P(None, "tp"), P(None, "tp"),
            P(None, "tp"), P(None, "tp"), P("fs", "sp", "tp"), P("tp"), P(None, "tp"),
            P("tp"), P("tp"), P("tp", None), P("tp", None),
        ),
        out_specs=(P("fs", ("sp", "tp"), None), P("fs", "sp", "tp")),
        check_vma=False,
    )
```

profile of v0, /device:TPU:23, one launch (start us, length us, event | category | flops | bytes accessed | tf_op | source)
XLA Modules:
  0.0 42.6 jit_solution(1096387825543756454)
XLA Ops:
  0.6 40.1 %shard_map.149 = (bf16[128,2048]{1,0:T(8,128)(2,1)}, f32[8,256]{1,0:T(8,128)}) custom-call(bf16[256,2048]{1,0:T(8,128)(2,1)} %bitcast.8, bf16[2048]{0:T(1024)(128)(2,1)} %ngain.1, bf16[8,256]{1,0:T(8,128)(2,1)} %bitcast.9, bf16[31,512]{1,0:T(8,128)(2,1)} %raw_taps.1, bf16[512]{0:T(512)(128)(2,1)} %gain_ref.1, bf16[512]{0:T(512)(128)(2,1)} %cgain_ref.1, ...), custom_call_target="tpu_custom_call" | custom-call | tf_op jit(solution)/shard_map/pallas_call | solution.py:327
  40.7 1.9 %shard_map.150 = (bf16[128,2048]{1,0:T(8,128)(2,1)}, f32[8,256]{1,0:T(8,128)}) custom-call(bf16[128,2048]{1,0:T(8,128)(2,1)} %get-tuple-element.6.mixed, f32[8,256]{1,0:T(8,128)} %get-tuple-element.7.mass_log), custom_call_target="tpu_custom_call" | custom-call | tf_op jit(solution)/shard_map/pallas_call | solution.py:369
where the time goes:
time: 42.8 us; the launch traced here: 42.6 us
  Pallas kernels  41.9 us (98%)
  between operations  0.64 us (1%)
    pallas_call x1, Pallas kernels, local(): pl.pallas_call(functools.partial(kernel, n, tp, taps, hp, chans * tp), ou...  40.1 us
    pallas_call x1, Pallas kernels, local(): pl.pallas_call(place, out_shape=(jax.ShapeDtypeStruct((share, model), bf1...  1.86 us

commit v1 on v0

v1 whole, which is shorter than its diff:
```python
import functools

import jax
import jax.numpy as jnp
from jax import lax
from jax.experimental import pallas as pl
from jax.experimental.pallas import tpu as pltpu
from jax.sharding import PartitionSpec as P

HEAD_DIM = 64

rms_eps = 1e-06
norm_eps = 1e-05
mass_floor = 0.01
HALO = 32
LANES = 128
LOG2E = 1.4426950408889634
MESH = pl.DeviceIdType.MESH


def kernel(
    n, tp, taps, total_channels,
    stream_hbm, ngain, offs, raw_taps, gain_ref, cgain_ref, cshift_ref,
    q_hbm, k_hbm, v_hbm, in_hbm, gate_hbm, attend_hbm, filter_hbm,
    out_ref, log_ref,
    stream, normed, weights, out_weights, packet, q_in, kv_in, offs_in, o_out, o_in, stat_out, stat_in,
    own_r, own_t, far_r, far_t, masses, off_rows, tap_ref, heads_ref, conv_ref, conv_share, leaving, arrived_ref,
    gated, halo, ext, filt, stats, stats_got,
    stream_sem, weight_sem, out_weight_sem, q_send, q_recv, kv_send, kv_recv, offs_send, offs_recv,
    o_send, o_recv, stat_send, stat_recv, out_send, out_recv, halo_send, halo_recv, chan_send, chan_recv,
):
    f32, bf16 = jnp.float32, jnp.bfloat16
    me = lax.axis_index("sp")
    core = lax.axis_index("tp")
    partner = 1 - core
    rows, model = normed.shape
    chans = in_hbm.shape[1]
    groups = packet.shape[1]
    slabs = chans // LANES
    lane = lax.broadcasted_iota(jnp.int32, (rows, LANES), 1)
    low = lane < HEAD_DIM

    def local_copy(src, dst, sem):
        return pltpu.make_async_copy(src, dst, sem)

    def send(src, dst, send_sem, recv_sem, to):
        return pltpu.make_async_remote_copy(
            src_ref=src, dst_ref=dst, send_sem=send_sem, recv_sem=recv_sem,
            device_id=to, device_id_type=MESH)

    projections = (q_hbm, k_hbm, v_hbm)
    first_order, other_order = (1, 2, 0), (0, 1, 2)

    def slot_of(t):
        return jnp.where(me == 0, first_order[t], other_order[t])

    def fetch(t):
        @pl.when(me == 0)
        def _():
            s = first_order[t]
            local_copy(projections[s], weights.at[s], weight_sem.at[s]).start()

        @pl.when(me != 0)
        def _():
            s = other_order[t]
            local_copy(projections[s], weights.at[s], weight_sem.at[s]).start()

    stream_copy = local_copy(stream_hbm, stream, stream_sem)
    gate_copies = [local_copy(w, weights.at[3 + t], weight_sem.at[3 + t]) for t, w in enumerate((in_hbm, gate_hbm))]
    out_copies = [local_copy(w, out_weights.at[t], out_weight_sem.at[t]) for t, w in enumerate((filter_hbm, attend_hbm))]
    stream_copy.start()
    fetch(0)
    fetch(1)

    barrier = pltpu.get_barrier_semaphore()
    peers = {0: (1,), 1: (0, 2, 3), 2: (1, 3), 3: (1, 2)}
    pl.semaphore_signal(barrier, inc=1, device_id={"tp": partner}, device_id_type=MESH)
    for d in range(n):
        @pl.when(me == d)
        def _(d=d):
            for p in peers[d]:
                pl.semaphore_signal(barrier, inc=1, device_id={"sp": p}, device_id_type=MESH)

    tap_ref[...] = jnp.zeros_like(tap_ref)
    for c in range(slabs):
        tap_ref[c, :taps] = raw_taps[:, c * LANES:(c + 1) * LANES].astype(f32)
    off_rows[0] = offs[...].astype(f32) * LOG2E
    masses[...] = jnp.zeros_like(masses)
    norm_gain = ngain[...].astype(f32).reshape(1, -1)
    band = min(64, rows)
    stream_copy.wait()

    @pl.loop(0, rows // band)
    def _(c):
        some = pl.ds(pl.multiple_of(c * band, band), band)
        x = stream[some, :].astype(f32)
        x = x * lax.rsqrt(jnp.mean(x * x, axis=-1, keepdims=True) + rms_eps)
        normed[some, :] = (x * norm_gain).astype(bf16)

    for d in range(n):
        @pl.when(me == d)
        def _(d=d):
            pl.semaphore_wait(barrier, len(peers[d]) + tp - 1)

    def q_copy(src_dev, dst_dev, g):
        return send(packet.at[0, g], q_in.at[src_dev - 2, g], q_send.at[dst_dev - 1, g],
                    q_recv.at[src_dev - 2, g], {"sp": dst_dev})

    def kv_copy(t, g):
        return send(packet.at[1 + t, g], kv_in.at[t, g], kv_send.at[t, g], kv_recv.at[t, g], {"sp": 1})

    offs_copy = send(offs, offs_in, offs_send, offs_recv, {"sp": 1})

    def o_copy(src_dev, dst_dev, g):
        return send(o_out.at[dst_dev - 2, g], o_in.at[src_dev - 1, g], o_send.at[dst_dev - 2, g],
                    o_recv.at[src_dev - 1, g], {"sp": dst_dev})

    def stat_copy(src_dev, dst_dev):
        return send(stat_out.at[dst_dev - 2], stat_in.at[src_dev - 1], stat_send.at[dst_dev - 2],
                    stat_recv.at[src_dev - 1], {"sp": dst_dev})

    @pl.when(me == 0)
    def _():
        offs_copy.start()

    wide = 2 * LANES
    halves = chans // wide

    def project(t, after):
        slot = slot_of(t)
        local_copy(q_hbm, weights.at[slot], weight_sem.at[slot]).wait()
        factor = jnp.where(slot == 0, LOG2E * HEAD_DIM ** (-0.5), 1.0).astype(f32)
        for half in range(halves):
            y = jnp.dot(normed[...], weights[slot, :, half * wide:(half + 1) * wide], preferred_element_type=f32)
            y = (y * factor).astype(bf16)
            for u in range(2):
                packet[slot, 2 * half + u] = y[:, u * LANES:(u + 1) * LANES]
            after(half)

    def after_first(half):
        @pl.when(me == 2)
        def _():
            for u in range(2):
                q_copy(2, 1, 2 * half + u).start()

        @pl.when(me == 3)
        def _():
            for u in range(2):
                q_copy(3, 1, 2 * half + u).start()
                q_copy(3, 2, 2 * half + u).start()

        if half == 0:
            @pl.when(me == 0)
            def _():
                kv_copy(0, 0).start()

    def after_second(half):
        if half == 0:
            @pl.when(me == 0)
            def _():
                kv_copy(1, 0).start()

    for copy in gate_copies:
        copy.start()
    project(0, after_first)
    fetch(2)
    project(1, after_second)
    for copy in out_copies:
        copy.start()
    for copy in gate_copies:
        copy.wait()

    @pl.loop(0, halves)
    def _(c):
        cols = pl.ds(pl.multiple_of(c * wide, wide), wide)
        x = normed[...]
        value = jnp.dot(x, weights[3, :, cols], preferred_element_type=f32).astype(bf16).astype(f32)
        gate = jnp.dot(x, weights[4, :, cols], preferred_element_type=f32).astype(bf16).astype(f32)
        g = (value * jax.nn.sigmoid(gate)).astype(bf16)
        gated[:, cols] = g[rows - HALO:]
        g = g.astype(f32)
        for u in range(2):
            ext[2 * c + u, HALO:, :] = g[:, u * LANES:(u + 1) * LANES]

    halo_copy = send(gated, halo, halo_send, halo_recv, {"sp": lax.rem(me + 1, n)})

    @pl.when(me < n - 1)
    def _():
        halo_copy.start()

    @pl.when(me == 0)
    def _():
        for g in range(1, groups):
            for t in range(2):
                if g == 1:
                    kv_copy(t, g).start()

    def after_third(half):
        pass

    project(2, after_third)

    @pl.when(me == 0)
    def _():
        for g in range(2, groups):
            for t in range(2):
                kv_copy(t, g).start()

    step = min(128, rows)

    def convolve(starts):
        @pl.loop(0, slabs)
        def _(c):
            for r0 in starts:
                acc = jnp.zeros((step, LANES), f32)
                for k in range(taps):
                    start = HALO - (taps - 1) + k + r0
                    acc = acc + ext[c, start:start + step, :] * tap_ref[c, k:k + 1, :]
                filt[c, r0:r0 + step, :] = acc

    chan_copy = send(stats, stats_got, chan_send, chan_recv, {"tp": partner})

    def convolve_first():
        @pl.when(me > 0)
        def _():
            halo_copy.wait_recv()
            for c in range(slabs):
                ext[c, :HALO, :] = halo[:, c * LANES:(c + 1) * LANES].astype(f32)

        @pl.when(me == 0)
        def _():
            for c in range(slabs):
                ext[c, :HALO, :] = jnp.zeros((HALO, LANES), f32)

        convolve([0])
        total = filt[0]
        for c in range(1, slabs):
            total = total + filt[c]
        lsum = jnp.sum(total, axis=1, keepdims=True)
        mean = lsum * (1.0 / chans)
        square = jnp.zeros((rows, LANES), f32)
        for c in range(slabs):
            dev = filt[c] - mean
            square = square + dev * dev
        lsq = jnp.sum(square, axis=1, keepdims=True)
        stats[...] = jnp.where(low, lsum, lsq)
        chan_copy.start()

    def channel_norm():
        chan_copy.wait()
        mine, other = stats[...], stats_got[...]
        mean = (mine[:, 0:1] + other[:, 0:1]) * (1.0 / total_channels)
        spread = jnp.zeros((rows, 1), f32)
        for s in (mine, other):
            apart = s[:, 0:1] * (1.0 / chans) - mean
            spread = spread + s[:, HEAD_DIM:HEAD_DIM + 1] + chans * apart * apart
        scale = lax.rsqrt(spread * (1.0 / total_channels) + norm_eps)
        for c in range(slabs):
            cols = slice(c * LANES, (c + 1) * LANES)
            y = (filt[c] - mean) * scale * cgain_ref[cols].astype(f32).reshape(1, -1) + cshift_ref[cols].astype(f32).reshape(1, -1)
            conv_ref[:, cols] = (y * jax.nn.sigmoid(y)).astype(bf16)

    tile = min(512, model)

    def conv_product():
        out_copies[0].wait()
        for c in range(0, model, tile):
            conv_share[:, c:c + tile] = jnp.dot(
                conv_ref[...], out_weights[0, :, c:c + tile], preferred_element_type=f32)

    ri = lax.broadcasted_iota(jnp.int32, (rows, rows), 0)
    ci = lax.broadcasted_iota(jnp.int32, (rows, rows), 1)
    tri = (ri >= ci).astype(bf16)

    def split_keys(k):
        zero = jnp.zeros_like(k)
        return jnp.where(low, k, zero), jnp.where(low, zero, k)

    def split_values(v):
        one = jnp.ones_like(v)
        return jnp.where(low, v, one), jnp.where(low, one, v)

    def attend(q, k, v, off, strict=None):
        z = lax.dot_general(q, k, (((1,), (1,)), ((), ())), preferred_element_type=f32) + off
        lose = jnp.maximum(z, jnp.log(1.0 + jnp.exp2(jnp.minimum(z, 100.0))) * LOG2E)
        if strict is not None:
            lose = jnp.where(strict, lose, 0.0)
        cum = jnp.dot(lose.astype(bf16), tri, preferred_element_type=f32)
        w = jnp.exp2(z - cum)
        if strict is not None:
            w = jnp.where(strict, w, 0.0)
        res = jnp.dot(w.astype(bf16), v, preferred_element_type=f32)
        return res, jnp.broadcast_to(cum[:, 0:1], (rows, LANES))

    def note(which, g, h, res, total):
        base = 0 if h else HEAD_DIM
        masses[which] = jnp.where(lane == base + g, res, jnp.where(lane == base + 4 + g, total, masses[which]))

    def pair(a, b):
        return jnp.where(low, a, b)

    @pl.loop(0, groups)
    def _(g):
        keys = split_keys(packet[1, g])
        values = split_values(packet[2, g])
        strict = ci < ri
        for h in range(2):
            res, total = attend(packet[0, g], keys[h], values[h], off_rows[0, pl.ds(2 * g + h, 1), :], strict)
            own_r[g, h] = res
            own_t[g, h] = jnp.exp2(-total)
            note(0, g, h, res, total)

        @pl.when(me == 1)
        def _():
            keys = split_keys(packet[1, g])
            values = split_values(packet[2, g])
            for i in (1, 0):
                send(packet.at[0, g], q_in.at[i, g], q_send.at[0, g], q_recv.at[i, g], {"sp": i + 2}).wait_recv()
                for h in range(2):
                    res, total = attend(q_in[i, g], keys[h], values[h], off_rows[0, pl.ds(2 * g + h, 1), :])
                    far_r[i, h] = res
                    far_t[i, h] = jnp.exp2(-total)

        @pl.when(me == 2)
        def _():
            keys = split_keys(packet[1, g])
            values = split_values(packet[2, g])
            send(packet.at[0, g], q_in.at[1, g], q_send.at[0, g], q_recv.at[1, g], {"sp": 3}).wait_recv()
            parts = []
            for h in range(2):
                res, total = attend(q_in[1, g], keys[h], values[h], off_rows[0, pl.ds(2 * g + h, 1), :])
                note(2, g, h, res, total)
                parts.append(res)
            o_out[1, g] = pair(*parts).astype(bf16)
            send(o_out.at[1, g], o_in.at[1, g], o_send.at[1, g], o_recv.at[1, g], {"sp": 3}).start()

        @pl.when(g == 0)
        def _():
            convolve(range(step, rows, step))

        @pl.when(g == 1)
        def _():
            convolve_first()

        @pl.when(g == 2)
        def _():
            channel_norm()

        @pl.when(g == 3)
        def _():
            conv_product()

        @pl.when(me == 1)
        def _():
            @pl.when(g == 0)
            def _():
                send(offs, offs_in, offs_send, offs_recv, {"sp": 0}).wait_recv()
                off_rows[1] = offs_in[...].astype(f32) * LOG2E

            for t in range(2):
                send(packet.at[1 + t, g], kv_in.at[t, g], kv_send.at[t, g], kv_recv.at[t, g], {"sp": 0}).wait_recv()
            keys = split_keys(kv_in[0, g])
            values = split_values(kv_in[1, g])
            for i in (1, 0):
                parts = []
                for h in range(2):
                    res, _ = attend(q_in[i, g], keys[h], values[h], off_rows[1, pl.ds(2 * g + h, 1), :])
                    res = far_r[i, h] + far_t[i, h] * res
                    note(1 + i, g, h, res, res)
                    parts.append(res)
                o_out[i, g] = pair(*parts).astype(bf16)
                send(o_out.at[i, g], o_in.at[0, g], o_send.at[i, g], o_recv.at[0, g], {"sp": i + 2}).start()
            for h in range(2):
                res, _ = attend(packet[0, g], keys[h], values[h], off_rows[1, pl.ds(2 * g + h, 1), :])
                res = own_r[g, h] + own_t[g, h] * res
                own_r[g, h] = res
                note(0, g, h, res, res)

    def stat_rows(which):
        t = jnp.transpose(masses[which])
        return jnp.concatenate([t[0:8], t[HEAD_DIM:HEAD_DIM + 8]], axis=0)

    @pl.when(me == 1)
    def _():
        for i in (1, 0):
            stat_out[i] = stat_rows(1 + i)
            stat_copy(1, i + 2).start()

    @pl.when(me == 2)
    def _():
        stat_out[1] = stat_rows(2)
        stat_copy(2, 3).start()

    blocks = (lax.broadcasted_iota(jnp.int32, (LANES, LANES), 0) // HEAD_DIM
              == lax.broadcasted_iota(jnp.int32, (LANES, LANES), 1) // HEAD_DIM).astype(bf16)

    @pl.when(me == 3)
    def _():
        stat_copy(2, 3).wait_recv()
        rest = jnp.zeros((LANES - 16, rows), f32)
        far_t[0, 0] = jnp.transpose(jnp.concatenate([stat_in[1], rest], axis=0))

    def finish(g):
        cols = slice(g * LANES, (g + 1) * LANES)

        def close(o):
            sq = jnp.dot((o * o).astype(bf16), blocks, preferred_element_type=f32)
            gain = gain_ref[cols].astype(f32).reshape(1, LANES)
            heads_ref[:, cols] = (o * lax.rsqrt(sq * (1.0 / HEAD_DIM) + rms_eps) * gain).astype(bf16)

        own = pair(own_r[g, 0], own_r[g, 1])

        @pl.when(me < 2)
        def _():
            close(own)

        @pl.when(me == 2)
        def _():
            through = pair(own_t[g, 0], own_t[g, 1])
            o_copy(1, 2, g).wait_recv()
            close(own + through * o_in[0, g].astype(f32))

        @pl.when(me == 3)
        def _():
            through = pair(own_t[g, 0], own_t[g, 1])
            tot = far_t[0, 0]
            middle = jnp.exp2(-pair(tot[:, 12 + g:13 + g], tot[:, 4 + g:5 + g]))
            send(o_out.at[1, g], o_in.at[1, g], o_send.at[1, g], o_recv.at[1, g], {"sp": 2}).wait_recv()
            send(o_out.at[1, g], o_in.at[0, g], o_send.at[1, g], o_recv.at[0, g], {"sp": 1}).wait_recv()
            close(own + through * (o_in[1, g].astype(f32) + middle * o_in[0, g].astype(f32)))

    out_copies[1].wait()
    early = groups // 2
    for g in range(early):
        finish(g)
    cut = early * LANES
    for c in range(0, model, tile):
        conv_share[:, c:c + tile] += jnp.dot(
            heads_ref[:, :cut], out_weights[1, :cut, c:c + tile], preferred_element_type=f32)
    for g in range(early, groups):
        finish(g)
    share = rows // tp
    theirs = pl.ds(pl.multiple_of(partner * share, share), share)
    ours = pl.ds(pl.multiple_of(core * share, share), share)
    leaves = []
    for c in range(0, model, tile):
        cols = slice(c, c + tile)
        leaving[:, cols] = (conv_share[theirs, cols] + jnp.dot(
            heads_ref[theirs, cut:], out_weights[1, cut:, cols], preferred_element_type=f32)).astype(bf16)
        copy = send(leaving.at[:, pl.ds(c, tile)], arrived_ref.at[:, pl.ds(c, tile)],
                    out_send.at[c // tile], out_recv.at[c // tile], {"tp": partner})
        copy.start()
        leaves.append(copy)

    mine = stat_rows(0)

    def write_log(m_odd, m_even):
        for g in range(groups):
            log_ref[2 * g:2 * g + 1] = jnp.log(jnp.maximum(m_even[g:g + 1], mass_floor))
            log_ref[2 * g + 1:2 * g + 2] = jnp.log(jnp.maximum(m_odd[g:g + 1], mass_floor))

    @pl.when(me < 2)
    def _():
        write_log(mine[0:4], mine[8:12])

    @pl.when(me == 2)
    def _():
        stat_copy(1, 2).wait_recv()
        far = stat_in[0]
        write_log(mine[0:4] + jnp.exp2(-mine[4:8]) * far[0:4], mine[8:12] + jnp.exp2(-mine[12:16]) * far[8:12])

    @pl.when(me == 3)
    def _():
        send(stat_out.at[1], stat_in.at[0], stat_send.at[1], stat_recv.at[0], {"sp": 1}).wait_recv()
        far, mid = stat_in[0], stat_in[1]
        odd = mid[0:4] + jnp.exp2(-mid[4:8]) * far[0:4]
        even = mid[8:12] + jnp.exp2(-mid[12:16]) * far[8:12]
        write_log(mine[0:4] + jnp.exp2(-mine[4:8]) * odd, mine[8:12] + jnp.exp2(-mine[12:16]) * even)

    for c in range(0, model, tile):
        cols = slice(c, c + tile)
        acc = conv_share[ours, cols] + jnp.dot(
            heads_ref[ours, cut:], out_weights[1, cut:, cols], preferred_element_type=f32)
        leaves[c // tile].wait()
        out_ref[:, cols] = (acc + arrived_ref[:, cols].astype(f32)).astype(bf16)

    @pl.when(me < n - 1)
    def _():
        halo_copy.wait_send()

    @pl.when(me == 0)
    def _():
        offs_copy.wait_send()
        for g in range(groups):
            for t in range(2):
                kv_copy(t, g).wait_send()

    @pl.when(me == 1)
    def _():
        for i in (1, 0):
            for g in range(groups):
                o_copy(1, i + 2, g).wait_send()
            stat_copy(1, i + 2).wait_send()

    @pl.when(me == 2)
    def _():
        for g in range(groups):
            q_copy(2, 1, g).wait_send()
            o_copy(2, 3, g).wait_send()
        stat_copy(2, 3).wait_send()

    @pl.when(me == 3)
    def _():
        for g in range(groups):
            q_copy(3, 1, g).wait_send()
            q_copy(3, 2, g).wait_send()


def place(mixed, mass_log, out_ref, log_ref, sem):
    copies = [
        pltpu.make_async_copy(mixed, out_ref, sem.at[0]),
        pltpu.make_async_copy(mass_log, log_ref, sem.at[1]),
    ]
    for copy in copies:
        copy.start()
    for copy in copies:
        copy.wait()


def local(n, tp,
    stream, norm_gain, query_weight, key_weight, value_weight, filter_input, filter_gate,
    score_offset, head_gain, filter_taps, channel_gain, channel_shift, attend_out, filter_out,
):
    f32, bf16 = jnp.float32, jnp.bfloat16
    rows = stream.shape[1]
    heads = score_offset.shape[2]
    groups = heads * HEAD_DIM // LANES
    chans = filter_input.shape[1]
    slabs = chans // LANES
    taps = filter_taps.shape[0]
    model = stream.shape[2]
    share = rows // tp
    tiles = model // min(512, model)

    vmem = pl.BlockSpec(memory_space=pltpu.VMEM)
    hbm = pl.BlockSpec(memory_space=pl.ANY)
    dma = pltpu.SemaphoreType.DMA
    mixed, mass_log = pl.pallas_call(
        functools.partial(kernel, n, tp, taps, chans * tp),
        out_shape=(
            jax.ShapeDtypeStruct((share, model), bf16),
            jax.ShapeDtypeStruct((heads, rows), f32),
        ),
        in_specs=[hbm] + [vmem] * 6 + [hbm] * 7,
        out_specs=(vmem,) * 2,
        scratch_shapes=[
            pltpu.VMEM((rows, model), bf16),
            pltpu.VMEM((rows, model), bf16),
            pltpu.VMEM((5, model, chans), bf16),
            pltpu.VMEM((2, chans, model), bf16),
            pltpu.VMEM((3, groups, rows, LANES), bf16),
            pltpu.VMEM((2, groups, rows, LANES), bf16),
            pltpu.VMEM((2, groups, rows, LANES), bf16),
            pltpu.VMEM((heads, rows), bf16),
            pltpu.VMEM((2, groups, rows, LANES), bf16),
            pltpu.VMEM((2, groups, rows, LANES), bf16),
            pltpu.VMEM((2, 16, rows), f32),
            pltpu.VMEM((2, 16, rows), f32),
            pltpu.VMEM((groups, 2, rows, LANES), f32),
            pltpu.VMEM((groups, 2, rows, LANES), f32),
            pltpu.VMEM((2, 2, rows, LANES), f32),
            pltpu.VMEM((2, 2, rows, LANES), f32),
            pltpu.VMEM((3, rows, LANES), f32),
            pltpu.VMEM((2, heads, rows), f32),
            pltpu.VMEM((slabs, taps + -taps % 8, LANES), f32),
            pltpu.VMEM((rows, heads * HEAD_DIM), bf16),
            pltpu.VMEM((rows, chans), bf16),
            pltpu.VMEM((rows, model), f32),
            pltpu.VMEM((share, model), bf16),
            pltpu.VMEM((share, model), bf16),
            pltpu.VMEM((HALO, chans), bf16),
            pltpu.VMEM((HALO, chans), bf16),
            pltpu.VMEM((slabs, HALO + rows, LANES), f32),
            pltpu.VMEM((slabs, rows, LANES), f32),
            pltpu.VMEM((rows, LANES), f32),
            pltpu.VMEM((rows, LANES), f32),
            dma, dma((5,)), dma((2,)), dma((2, groups)), dma((2, groups)), dma((2, groups)), dma((2, groups)), dma, dma,
            dma((2, groups)), dma((2, groups)), dma((2,)), dma((2,)), dma((tiles,)), dma((tiles,)), dma, dma, dma, dma,
        ],
        compiler_params=pltpu.CompilerParams(
            collective_id=0, has_side_effects=True, vmem_limit_bytes=56 * 1024 * 1024),
    )(stream[0], norm_gain, score_offset[0].T, filter_taps, head_gain, channel_gain, channel_shift,
      query_weight, key_weight, value_weight, filter_input, filter_gate, attend_out, filter_out)
    mixed, mass_log = pl.pallas_call(
        place,
        out_shape=(
            jax.ShapeDtypeStruct((share, model), bf16),
            jax.ShapeDtypeStruct((heads, rows), f32),
        ),
        in_specs=[vmem] * 2,
        out_specs=(hbm,) * 2,
        scratch_shapes=[dma((2,))],
    )(mixed, mass_log)
    return (mixed[None], mass_log.T[None])


def shifted(value, axis, steps):
    count = lax.axis_size(axis)
    first, last = (max(0, -steps), min(count, count - steps))
    return lax.ppermute(value, axis, [(source, source + steps) for source in range(first, last)])


def local_ring(
    stream,
    norm_gain,
    query_weight,
    key_weight,
    value_weight,
    filter_input,
    filter_gate,
    score_offset,
    head_gain,
    filter_taps,
    channel_gain,
    channel_shift,
    attend_out,
    filter_out,
):
    rows_here = stream.shape[1]
    total_channels = filter_input.shape[1] * lax.axis_size("tp")
    xfloat = stream[0].astype(jnp.float32)
    normed = xfloat * lax.rsqrt(jnp.mean(xfloat * xfloat, axis=-1, keepdims=True) + rms_eps)
    normed = (normed * norm_gain.astype(jnp.float32)).astype(jnp.bfloat16)

    def project(weight):
        return jnp.dot(normed, weight, preferred_element_type=jnp.float32).astype(jnp.bfloat16)

    queries = project(query_weight)
    keys_here = project(key_weight)
    values_here = project(value_weight)
    conv_in = project(filter_input)
    conv_gate = project(filter_gate)
    offsets_here = score_offset[0]
    heads_here = offsets_here.shape[1]
    first_pos = lax.axis_index("sp") * rows_here
    position = first_pos + jnp.arange(rows_here, dtype=jnp.int32)
    qheads = queries.reshape(rows_here, heads_here, HEAD_DIM)

    def absorb(state_now, kblock, vblock, oblock, first_key):
        attended, weight_mass, survive = state_now
        span = kblock.shape[0]
        kblock = kblock.reshape(span, heads_here, HEAD_DIM)
        vblock = vblock.reshape(span, heads_here, HEAD_DIM)
        scores = jnp.einsum(
            "thd,shd->hts", qheads, kblock, preferred_element_type=jnp.float32
        ) * HEAD_DIM ** (-0.5)
        scores = scores + oblock.astype(jnp.float32).T[:, None, :]
        key_pos = first_key + jnp.arange(span, dtype=jnp.int32)
        strict = ((key_pos[None, :] < position[:, None]) & (key_pos[None, :] >= 0))[None]
        losing = jnp.where(strict, jax.nn.log_sigmoid(-scores), 0.0)
        beyond = lax.cumsum(losing, axis=2, reverse=True) - losing + survive[:, :, None]
        weights = jnp.where(strict, jnp.exp(jax.nn.log_sigmoid(scores) + beyond), 0.0)
        weight_mass = weight_mass + jnp.sum(weights, axis=2)
        attended = attended + jnp.einsum(
            "hts,shd->thd", weights.astype(jnp.bfloat16), vblock, preferred_element_type=jnp.float32
        )
        survive = survive + jnp.sum(losing, axis=2)
        return (attended, weight_mass, survive)

    initial = (
        jnp.zeros((rows_here, heads_here, HEAD_DIM), jnp.float32),
        jnp.zeros((heads_here, rows_here), jnp.float32),
        jnp.zeros((heads_here, rows_here), jnp.float32),
    )
    state_now = absorb(initial, keys_here, values_here, offsets_here, first_pos)

    def pass_turn(turn_index, carried):
        state_now, travelling = carried
        travelling = shifted((travelling[0], travelling[1], travelling[2]), "sp", 1)
        first_key = first_pos - (turn_index + 1) * rows_here
        state_now = absorb(state_now, travelling[0], travelling[1], travelling[2], first_key)
        return (state_now, travelling)

    state_now, travelling = lax.fori_loop(
        0, lax.axis_size("sp") - 1, pass_turn, (state_now, (keys_here, values_here, offsets_here))
    )
    attended, weight_mass, survive = state_now
    head_scale = lax.rsqrt(jnp.mean(attended * attended, axis=-1, keepdims=True) + rms_eps)
    heads_flat = attended * head_scale * head_gain.astype(jnp.float32).reshape(heads_here, HEAD_DIM)
    heads_flat = heads_flat.astype(jnp.bfloat16).reshape(rows_here, heads_here * HEAD_DIM)
    mass_log = jnp.log(jnp.maximum(weight_mass.T, mass_floor))
    gated_rows = (
        conv_in.astype(jnp.float32) * jax.nn.sigmoid(conv_gate.astype(jnp.float32))
    ).astype(jnp.bfloat16)
    reach_back = filter_taps.shape[0] - 1
    earlier = shifted(gated_rows[rows_here - reach_back :], "sp", 1)
    extended = jnp.concatenate([earlier, gated_rows], axis=0).astype(jnp.float32)
    tap_values = filter_taps.astype(jnp.float32)
    filtered = jnp.zeros((rows_here, gated_rows.shape[1]), jnp.float32)
    for tap_index in range(reach_back + 1):
        filtered = filtered + extended[tap_index : tap_index + rows_here] * tap_values[tap_index]
    center = lax.psum(jnp.sum(filtered, axis=-1), "tp") / total_channels
    deviation = filtered - center[:, None]
    spread = lax.psum(jnp.sum(deviation * deviation, axis=-1), "tp") / total_channels
    conv_out = jax.nn.silu(
        deviation * lax.rsqrt(spread[:, None] + norm_eps) * channel_gain.astype(jnp.float32)
        + channel_shift.astype(jnp.float32)
    ).astype(jnp.bfloat16)
    mixed_out = lax.psum_scatter(
        (
            jnp.dot(heads_flat, attend_out, preferred_element_type=jnp.float32)
            + jnp.dot(conv_out, filter_out, preferred_element_type=jnp.float32)
        ).astype(jnp.bfloat16),
        "tp",
        scatter_dimension=0,
        tiled=True,
    )
    return (mixed_out[None], mass_log[None])


def solution(mesh):
    n, tp = mesh.shape["sp"], mesh.shape["tp"]

    def choose(*args):
        rows, heads, chans = args[0].shape[1], args[7].shape[2], args[5].shape[1]
        same = args[2].shape[1] == chans and heads * HEAD_DIM == 4 * LANES == chans
        if n == 4 and tp == 2 and same and rows % 128 == 0:
            return local(n, tp, *args)
        return local_ring(*args)

    return jax.shard_map(
        choose,
        mesh=mesh,
        in_specs=(
            P("fs", "sp", None), P(), P(None, "tp"), P(None, "tp"), P(None, "tp"),
            P(None, "tp"), P(None, "tp"), P("fs", "sp", "tp"), P("tp"), P(None, "tp"),
            P("tp"), P("tp"), P("tp", None), P("tp", None),
        ),
        out_specs=(P("fs", ("sp", "tp"), None), P("fs", "sp", "tp")),
        check_vma=False,
    )
```

time: 42.8 us -> 37.4 us (0.87)
  Pallas kernels: 41.9 us -> 36.5 us
    pallas_call x1, Pallas kernels: 40.1 us -> 34.7 us  [local(): pl.pallas_call(functools.partial(kernel, n, tp, taps, chans * tp), out_sh...]
where the time goes in v1:
time: 37.4 us; the launch traced here: 37.2 us
  Pallas kernels  36.5 us (98%)
  between operations  0.64 us (2%)
    pallas_call x1, Pallas kernels, local(): pl.pallas_call(functools.partial(kernel, n, tp, taps, chans * tp), out_sh...  34.7 us
    pallas_call x1, Pallas kernels, local(): pl.pallas_call(place, out_shape=(jax.ShapeDtypeStruct((share, model), bf1...  1.86 us

profile of v1, /device:TPU:23, one launch (start us, length us, event | category | flops | bytes accessed | tf_op | source)
XLA Modules:
  0.0 37.2 jit_solution(2763309973228859448)
XLA Ops:
  0.6 34.7 %shard_map.149 = (bf16[128,2048]{1,0:T(8,128)(2,1)}, f32[8,256]{1,0:T(8,128)}) custom-call(bf16[256,2048]{1,0:T(8,128)(2,1)} %bitcast.8, bf16[2048]{0:T(1024)(128)(2,1)} %ngain.1, bf16[8,256]{1,0:T(8,128)(2,1)} %bitcast.9, bf16[31,512]{1,0:T(8,128)(2,1)} %raw_taps.1, bf16[512]{0:T(512)(128)(2,1)} %gain_ref.1, bf16[512]{0:T(512)(128)(2,1)} %cgain_ref.1, ...), custom_call_target="tpu_custom_call" | custom-call | tf_op jit(solution)/shard_map/pallas_call | solution.py:548
  35.3 1.9 %shard_map.150 = (bf16[128,2048]{1,0:T(8,128)(2,1)}, f32[8,256]{1,0:T(8,128)}) custom-call(bf16[128,2048]{1,0:T(8,128)(2,1)} %get-tuple-element.6.mixed, f32[8,256]{1,0:T(8,128)} %get-tuple-element.7.mass_log), custom_call_target="tpu_custom_call" | custom-call | tf_op jit(solution)/shard_map/pallas_call | solution.py:594

commit v2 on v1

--- a/solution.py
+++ b/solution.py
@@ -280,17 +280,27 @@
         one = jnp.ones_like(v)
         return jnp.where(low, v, one), jnp.where(low, one, v)
 
-    def attend(q, k, v, off, strict=None):
+    strict = ci < ri
+
+    def attend(blocks_q, k, v, off, own_first):
+        q = jnp.concatenate(blocks_q, axis=0)
         z = lax.dot_general(q, k, (((1,), (1,)), ((), ())), preferred_element_type=f32) + off
         lose = jnp.maximum(z, jnp.log(1.0 + jnp.exp2(jnp.minimum(z, 100.0))) * LOG2E)
-        if strict is not None:
-            lose = jnp.where(strict, lose, 0.0)
-        cum = jnp.dot(lose.astype(bf16), tri, preferred_element_type=f32)
-        w = jnp.exp2(z - cum)
-        if strict is not None:
-            w = jnp.where(strict, w, 0.0)
+
+        def masked(x):
+            if not own_first:
+                return x
+            head = jnp.where(strict, x[:rows], 0.0)
+            return jnp.concatenate([head, x[rows:]], axis=0) if len(blocks_q) > 1 else head
+
+        cum = jnp.dot(masked(lose).astype(bf16), tri, preferred_element_type=f32)
+        w = masked(jnp.exp2(z - cum))
         res = jnp.dot(w.astype(bf16), v, preferred_element_type=f32)
-        return res, jnp.broadcast_to(cum[:, 0:1], (rows, LANES))
+        pieces = []
+        for r in range(len(blocks_q)):
+            some = slice(r * rows, (r + 1) * rows)
+            pieces.append((res[some], jnp.broadcast_to(cum[some, 0:1], (rows, LANES))))
+        return pieces
 
     def note(which, g, h, res, total):
         base = 0 if h else HEAD_DIM
@@ -299,39 +309,44 @@
     def pair(a, b):
         return jnp.where(low, a, b)
 
-    @pl.loop(0, groups)
-    def _(g):
+    def near_blocks(g, others):
         keys = split_keys(packet[1, g])
         values = split_values(packet[2, g])
-        strict = ci < ri
+        rest = []
         for h in range(2):
-            res, total = attend(packet[0, g], keys[h], values[h], off_rows[0, pl.ds(2 * g + h, 1), :], strict)
+            first, *more = attend([packet[0, g]] + others, keys[h], values[h], off_rows[0, pl.ds(2 * g + h, 1), :], True)
+            res, total = first
             own_r[g, h] = res
             own_t[g, h] = jnp.exp2(-total)
             note(0, g, h, res, total)
+            rest.append(more)
+        return rest
+
+    @pl.loop(0, groups)
+    def _(g):
+        @pl.when(((me == 0) | (me == 3)) & (g % 2 == 0))
+        def _():
+            for u in range(2):
+                near_blocks(g + u, [])
 
         @pl.when(me == 1)
         def _():
-            keys = split_keys(packet[1, g])
-            values = split_values(packet[2, g])
             for i in (1, 0):
                 send(packet.at[0, g], q_in.at[i, g], q_send.at[0, g], q_recv.at[i, g], {"sp": i + 2}).wait_recv()
-                for h in range(2):
-                    res, total = attend(q_in[i, g], keys[h], values[h], off_rows[0, pl.ds(2 * g + h, 1), :])
+            rest = near_blocks(g, [q_in[1, g], q_in[0, g]])
+            for h in range(2):
+                for i in (1, 0):
+                    res, total = rest[h][1 - i]
                     far_r[i, h] = res
                     far_t[i, h] = jnp.exp2(-total)
 
         @pl.when(me == 2)
         def _():
-            keys = split_keys(packet[1, g])
-            values = split_values(packet[2, g])
             send(packet.at[0, g], q_in.at[1, g], q_send.at[0, g], q_recv.at[1, g], {"sp": 3}).wait_recv()
-            parts = []
+            rest = near_blocks(g, [q_in[1, g]])
             for h in range(2):
-                res, total = attend(q_in[1, g], keys[h], values[h], off_rows[0, pl.ds(2 * g + h, 1), :])
-                note(2, g, h, res, total)
-                parts.append(res)
-            o_out[1, g] = pair(*parts).astype(bf16)
+                note(2, g, h, *rest[h][0])
+            o_out[1, g] = pair(rest[0][0][0], rest[1][0][0]).astype(bf16)
             send(o_out.at[1, g], o_in.at[1, g], o_send.at[1, g], o_recv.at[1, g], {"sp": 3}).start()
 
         @pl.when(g == 0)
@@ -361,20 +376,21 @@
                 send(packet.at[1 + t, g], kv_in.at[t, g], kv_send.at[t, g], kv_recv.at[t, g], {"sp": 0}).wait_recv()
             keys = split_keys(kv_in[0, g])
             values = split_values(kv_in[1, g])
-            for i in (1, 0):
-                parts = []
-                for h in range(2):
-                    res, _ = attend(q_in[i, g], keys[h], values[h], off_rows[1, pl.ds(2 * g + h, 1), :])
-                    res = far_r[i, h] + far_t[i, h] * res
+            parts = [[], []]
+            for h in range(2):
+                pieces = attend([q_in[1, g], q_in[0, g], packet[0, g]], keys[h], values[h],
+                                off_rows[1, pl.ds(2 * g + h, 1), :], False)
+                for i in (1, 0):
+                    res = far_r[i, h] + far_t[i, h] * pieces[1 - i][0]
                     note(1 + i, g, h, res, res)
-                    parts.append(res)
-                o_out[i, g] = pair(*parts).astype(bf16)
-                send(o_out.at[i, g], o_in.at[0, g], o_send.at[i, g], o_recv.at[0, g], {"sp": i + 2}).start()
-            for h in range(2):
-                res, _ = attend(packet[0, g], keys[h], values[h], off_rows[1, pl.ds(2 * g + h, 1), :])
-                res = own_r[g, h] + own_t[g, h] * res
+                    parts[i].append(res)
+                res = own_r[g, h] + own_t[g, h] * pieces[2][0]
                 own_r[g, h] = res
                 note(0, g, h, res, res)
+            for i in (1, 0):
+                o_out[i, g] = pair(*parts[i]).astype(bf16)
+            for i in (1, 0):
+                send(o_out.at[i, g], o_in.at[0, g], o_send.at[i, g], o_recv.at[0, g], {"sp": i + 2}).start()
 
     def stat_rows(which):
         t = jnp.transpose(masses[which])

time: 37.4 us -> 32.5 us (0.87)
  Pallas kernels: 36.5 us -> 31.7 us
    pallas_call x1, Pallas kernels: 34.7 us -> 29.8 us  [local(): pl.pallas_call(functools.partial(kernel, n, tp, taps, chans * tp), out_sh...]
where the time goes in v2:
time: 32.5 us; the launch traced here: 32.3 us
  Pallas kernels  31.7 us (98%)
  between operations  0.64 us (2%)
    pallas_call x1, Pallas kernels, local(): pl.pallas_call(functools.partial(kernel, n, tp, taps, chans * tp), out_sh...  29.8 us
    pallas_call x1, Pallas kernels, local(): pl.pallas_call(place, out_shape=(jax.ShapeDtypeStruct((share, model), bf1...  1.86 us

profile of v2, /device:TPU:23, one launch (start us, length us, event | category | flops | bytes accessed | tf_op | source)
XLA Modules:
  0.0 32.3 jit_solution(8074158641770813632)
XLA Ops:
  0.6 29.8 %shard_map.149 = (bf16[128,2048]{1,0:T(8,128)(2,1)}, f32[8,256]{1,0:T(8,128)}) custom-call(bf16[256,2048]{1,0:T(8,128)(2,1)} %bitcast.8, bf16[2048]{0:T(1024)(128)(2,1)} %ngain.1, bf16[8,256]{1,0:T(8,128)(2,1)} %bitcast.9, bf16[31,512]{1,0:T(8,128)(2,1)} %raw_taps.1, bf16[512]{0:T(512)(128)(2,1)} %gain_ref.1, bf16[512]{0:T(512)(128)(2,1)} %cgain_ref.1, ...), custom_call_target="tpu_custom_call" | custom-call | tf_op jit(solution)/shard_map/pallas_call | solution.py:564
  30.5 1.9 %shard_map.150 = (bf16[128,2048]{1,0:T(8,128)(2,1)}, f32[8,256]{1,0:T(8,128)}) custom-call(bf16[128,2048]{1,0:T(8,128)(2,1)} %get-tuple-element.6.mixed, f32[8,256]{1,0:T(8,128)} %get-tuple-element.7.mass_log), custom_call_target="tpu_custom_call" | custom-call | tf_op jit(solution)/shard_map/pallas_call | solution.py:610

commit v3 on v2

--- a/solution.py
+++ b/solution.py
@@ -20,13 +20,14 @@
 
 def kernel(
     n, tp, taps, total_channels,
-    stream_hbm, ngain, offs, raw_taps, gain_ref, cgain_ref, cshift_ref,
+    stream_hbm, ngain_hbm, offs_hbm, taps_hbm, gain_hbm, cgain_hbm, cshift_hbm,
     q_hbm, k_hbm, v_hbm, in_hbm, gate_hbm, attend_hbm, filter_hbm,
-    out_ref, log_ref,
+    out_hbm, log_hbm,
+    ngain, offs, raw_taps, gain_ref, cgain_ref, cshift_ref, out_ref, log_ref,
     stream, normed, weights, out_weights, packet, q_in, kv_in, offs_in, o_out, o_in, stat_out, stat_in,
     own_r, own_t, far_r, far_t, masses, off_rows, tap_ref, heads_ref, conv_ref, conv_share, leaving, arrived_ref,
     gated, halo, ext, filt, stats, stats_got,
-    stream_sem, weight_sem, out_weight_sem, q_send, q_recv, kv_send, kv_recv, offs_send, offs_recv,
+    small_sem, place_sem, stream_sem, weight_sem, out_weight_sem, q_send, q_recv, kv_send, kv_recv, kv_last_send, kv_last_recv, offs_send, offs_recv,
     o_send, o_recv, stat_send, stat_recv, out_send, out_recv, halo_send, halo_recv, chan_send, chan_recv,
 ):
     f32, bf16 = jnp.float32, jnp.bfloat16
@@ -54,26 +55,40 @@
     def slot_of(t):
         return jnp.where(me == 0, first_order[t], other_order[t])
 
-    def fetch(t):
-        @pl.when(me == 0)
-        def _():
-            s = first_order[t]
-            local_copy(projections[s], weights.at[s], weight_sem.at[s]).start()
-
-        @pl.when(me != 0)
-        def _():
-            s = other_order[t]
-            local_copy(projections[s], weights.at[s], weight_sem.at[s]).start()
-
-    stream_copy = local_copy(stream_hbm, stream, stream_sem)
-    gate_copies = [local_copy(w, weights.at[3 + t], weight_sem.at[3 + t]) for t, w in enumerate((in_hbm, gate_hbm))]
+    wide = 2 * LANES
+    halves = chans // wide
+
+    def weight_copy(w, slot, half):
+        cols = pl.ds(half * wide, wide)
+        return local_copy(w.at[:, cols], weights.at[slot, :, cols], weight_sem.at[slot, half])
+
+    def fetch(t, half):
+        for order, here in ((first_order, me == 0), (other_order, me != 0)):
+            @pl.when(here)
+            def _(s=order[t]):
+                weight_copy(projections[s], s, half).start()
+
+    band = min(64, rows)
+
+    def stream_copy(c):
+        some = pl.ds(pl.multiple_of(c * band, band), band)
+        return local_copy(stream_hbm.at[some], stream.at[some], stream_sem.at[c])
+
+    small = [local_copy(a, b, small_sem.at[t]) for t, (a, b) in enumerate((
+        (ngain_hbm, ngain), (offs_hbm, offs), (taps_hbm, raw_taps), (gain_hbm, gain_ref),
+        (cgain_hbm, cgain_ref), (cshift_hbm, cshift_ref)))]
+    gate_copies = [weight_copy(w, 3 + t, half) for half in range(halves) for t, w in enumerate((in_hbm, gate_hbm))]
     out_copies = [local_copy(w, out_weights.at[t], out_weight_sem.at[t]) for t, w in enumerate((filter_hbm, attend_hbm))]
-    stream_copy.start()
-    fetch(0)
-    fetch(1)
+    for c in range(rows // band):
+        stream_copy(c).start()
+    small[0].start()
+    for t in range(2):
+        fetch(t, 0)
+    for copy in small[1:]:
+        copy.start()
 
     barrier = pltpu.get_barrier_semaphore()
-    peers = {0: (1,), 1: (0, 2, 3), 2: (1, 3), 3: (1, 2)}
+    peers = {0: (1, 2), 1: (0, 2, 3), 2: (0, 1, 3), 3: (1, 2)}
     pl.semaphore_signal(barrier, inc=1, device_id={"tp": partner}, device_id_type=MESH)
     for d in range(n):
         @pl.when(me == d)
@@ -81,92 +96,117 @@
             for p in peers[d]:
                 pl.semaphore_signal(barrier, inc=1, device_id={"sp": p}, device_id_type=MESH)
 
+    small[0].wait()
+    norm_gain = ngain[...].astype(f32).reshape(1, -1)
+
+    @pl.loop(0, rows // band)
+    def _(c):
+        stream_copy(c).wait()
+
+        @pl.when(c == 0)
+        def _():
+            for half in range(1, halves):
+                for t in range(2):
+                    fetch(t, half)
+            for copy in gate_copies:
+                copy.start()
+
+        some = pl.ds(pl.multiple_of(c * band, band), band)
+        x = stream[some, :].astype(f32)
+        x = x * lax.rsqrt(jnp.mean(x * x, axis=-1, keepdims=True) + rms_eps)
+        normed[some, :] = (x * norm_gain).astype(bf16)
+
+    for half in range(halves):
+        fetch(2, half)
+    for copy in small[1:]:
+        copy.wait()
+
+    for d in range(n):
+        @pl.when(me == d)
+        def _(d=d):
+            pl.semaphore_wait(barrier, len(peers[d]) + tp - 1)
+
+    def q_copy(src_dev, dst_dev, g):
+        return send(packet.at[0, g], q_in.at[src_dev - 2, g], q_send.at[dst_dev - 1, g],
+                    q_recv.at[src_dev - 2, g], {"sp": dst_dev})
+
+    last = groups - 1
+
+    def kv_copy(t, g):
+        return send(packet.at[1 + t, g], kv_in.at[t, g], kv_send.at[t, g], kv_recv.at[t, g], {"sp": 1})
+
+    def kv_last(t, src_dev):
+        return send(packet.at[1 + t, last], kv_in.at[t, 0 if src_dev else last],
+                    kv_last_send.at[t], kv_last_recv.at[t, src_dev], {"sp": 2})
+
+    def offs_copy(src_dev, dst_dev):
+        return send(offs, offs_in.at[src_dev], offs_send.at[dst_dev - 1], offs_recv.at[src_dev], {"sp": dst_dev})
+
+    def o_copy(src_dev, dst_dev, g):
+        return send(o_out.at[dst_dev - 2, g], o_in.at[src_dev - 1, g], o_send.at[dst_dev - 2, g],
+                    o_recv.at[src_dev - 1, g], {"sp": dst_dev})
+
+    def stat_copy(src_dev, dst_dev):
+        return send(stat_out.at[dst_dev - 2], stat_in.at[src_dev - 1], stat_send.at[dst_dev - 2],
+                    stat_recv.at[src_dev - 1], {"sp": dst_dev})
+
+    @pl.when(me == 0)
+    def _():
+        offs_copy(0, 1).start()
+        offs_copy(0, 2).start()
+
+    @pl.when(me == 1)
+    def _():
+        offs_copy(1, 2).start()
+
+    def keep(slot, half, y):
+        factor = jnp.where(slot == 0, LOG2E * HEAD_DIM ** (-0.5), 1.0).astype(f32)
+        y = (y * factor).astype(bf16)
+        for u in range(2):
+            packet[slot, 2 * half + u] = y[:, u * LANES:(u + 1) * LANES]
+
+    def project(jobs):
+        for t, half in jobs:
+            slot = slot_of(t)
+            weight_copy(q_hbm, slot, half).wait()
+        for t, half in jobs:
+            slot = slot_of(t)
+            keep(slot, half, jnp.dot(
+                normed[...], weights[slot, :, half * wide:(half + 1) * wide], preferred_element_type=f32))
+
+    for half in range(halves):
+        project([(0, half), (1, half)])
+
+        @pl.when(me == 0)
+        def _():
+            if half == 0:
+                kv_copy(0, 0).start()
+                kv_copy(1, 0).start()
+
+        @pl.when(me == 2)
+        def _():
+            for g in (2 * half, 2 * half + 1):
+                if g < last:
+                    q_copy(2, 1, g).start()
+
+        @pl.when(me == 3)
+        def _():
+            if half > 0:
+                q_copy(3, 2, 2 * half - 1).start()
+            q_copy(3, 1, 2 * half).start()
+            q_copy(3, 2, 2 * half).start()
+            if 2 * half + 1 < last:
+                q_copy(3, 1, 2 * half + 1).start()
+            else:
+                q_copy(3, 2, 2 * half + 1).start()
+
+    for copy in out_copies:
+        copy.start()
     tap_ref[...] = jnp.zeros_like(tap_ref)
     for c in range(slabs):
         tap_ref[c, :taps] = raw_taps[:, c * LANES:(c + 1) * LANES].astype(f32)
     off_rows[0] = offs[...].astype(f32) * LOG2E
     masses[...] = jnp.zeros_like(masses)
-    norm_gain = ngain[...].astype(f32).reshape(1, -1)
-    band = min(64, rows)
-    stream_copy.wait()
-
-    @pl.loop(0, rows // band)
-    def _(c):
-        some = pl.ds(pl.multiple_of(c * band, band), band)
-        x = stream[some, :].astype(f32)
-        x = x * lax.rsqrt(jnp.mean(x * x, axis=-1, keepdims=True) + rms_eps)
-        normed[some, :] = (x * norm_gain).astype(bf16)
-
-    for d in range(n):
-        @pl.when(me == d)
-        def _(d=d):
-            pl.semaphore_wait(barrier, len(peers[d]) + tp - 1)
-
-    def q_copy(src_dev, dst_dev, g):
-        return send(packet.at[0, g], q_in.at[src_dev - 2, g], q_send.at[dst_dev - 1, g],
-                    q_recv.at[src_dev - 2, g], {"sp": dst_dev})
-
-    def kv_copy(t, g):
-        return send(packet.at[1 + t, g], kv_in.at[t, g], kv_send.at[t, g], kv_recv.at[t, g], {"sp": 1})
-
-    offs_copy = send(offs, offs_in, offs_send, offs_recv, {"sp": 1})
-
-    def o_copy(src_dev, dst_dev, g):
-        return send(o_out.at[dst_dev - 2, g], o_in.at[src_dev - 1, g], o_send.at[dst_dev - 2, g],
-                    o_recv.at[src_dev - 1, g], {"sp": dst_dev})
-
-    def stat_copy(src_dev, dst_dev):
-        return send(stat_out.at[dst_dev - 2], stat_in.at[src_dev - 1], stat_send.at[dst_dev - 2],
-                    stat_recv.at[src_dev - 1], {"sp": dst_dev})
-
-    @pl.when(me == 0)
-    def _():
-        offs_copy.start()
-
-    wide = 2 * LANES
-    halves = chans // wide
-
-    def project(t, after):
-        slot = slot_of(t)
-        local_copy(q_hbm, weights.at[slot], weight_sem.at[slot]).wait()
-        factor = jnp.where(slot == 0, LOG2E * HEAD_DIM ** (-0.5), 1.0).astype(f32)
-        for half in range(halves):
-            y = jnp.dot(normed[...], weights[slot, :, half * wide:(half + 1) * wide], preferred_element_type=f32)
-            y = (y * factor).astype(bf16)
-            for u in range(2):
-                packet[slot, 2 * half + u] = y[:, u * LANES:(u + 1) * LANES]
-            after(half)
-
-    def after_first(half):
-        @pl.when(me == 2)
-        def _():
-            for u in range(2):
-                q_copy(2, 1, 2 * half + u).start()
-
-        @pl.when(me == 3)
-        def _():
-            for u in range(2):
-                q_copy(3, 1, 2 * half + u).start()
-                q_copy(3, 2, 2 * half + u).start()
-
-        if half == 0:
-            @pl.when(me == 0)
-            def _():
-                kv_copy(0, 0).start()
-
-    def after_second(half):
-        if half == 0:
-            @pl.when(me == 0)
-            def _():
-                kv_copy(1, 0).start()
-
-    for copy in gate_copies:
-        copy.start()
-    project(0, after_first)
-    fetch(2)
-    project(1, after_second)
-    for copy in out_copies:
-        copy.start()
     for copy in gate_copies:
         copy.wait()
 
@@ -190,21 +230,20 @@
 
     @pl.when(me == 0)
     def _():
-        for g in range(1, groups):
-            for t in range(2):
-                if g == 1:
-                    kv_copy(t, g).start()
-
-    def after_third(half):
-        pass
-
-    project(2, after_third)
-
-    @pl.when(me == 0)
-    def _():
-        for g in range(2, groups):
+        for g in range(1, last):
             for t in range(2):
                 kv_copy(t, g).start()
+        for t in range(2):
+            kv_last(t, 0).start()
+        for t in range(2):
+            kv_copy(t, last).start()
+
+    project([(2, half) for half in range(halves)])
+
+    @pl.when(me == 1)
+    def _():
+        for t in range(2):
+            kv_last(t, 1).start()
 
     step = min(128, rows)
 
@@ -260,7 +299,7 @@
             y = (filt[c] - mean) * scale * cgain_ref[cols].astype(f32).reshape(1, -1) + cshift_ref[cols].astype(f32).reshape(1, -1)
             conv_ref[:, cols] = (y * jax.nn.sigmoid(y)).astype(bf16)
 
-    tile = min(512, model)
+    tile = min(1024, model)
 
     def conv_product():
         out_copies[0].wait()
@@ -322,28 +361,58 @@
             rest.append(more)
         return rest
 
-    @pl.loop(0, groups)
+    convolve(range(step, rows, step))
+
+    @pl.when(me != 2)
+    def _():
+        @pl.loop(0, groups // 2)
+        def _(half):
+            for u in range(2):
+                near_blocks(2 * half + u, [])
+
+    convolve_first()
+
+    def q_from(src_dev, dst_dev, g):
+        return send(packet.at[0, g], q_in.at[src_dev - 2, g], q_send.at[dst_dev - 1, g],
+                    q_recv.at[src_dev - 2, g], {"sp": src_dev})
+
+    def kv_from(t, g):
+        return send(packet.at[1 + t, g], kv_in.at[t, g], kv_send.at[t, g], kv_recv.at[t, g], {"sp": 0})
+
+    @pl.when(me == 1)
+    def _():
+        offs_copy_back = send(offs, offs_in.at[0], offs_send.at[0], offs_recv.at[0], {"sp": 0})
+        offs_copy_back.wait_recv()
+        off_rows[1] = offs_in[0].astype(f32) * LOG2E
+
+    @pl.when(me == 2)
+    def _():
+        for src in range(2):
+            send(offs, offs_in.at[src], offs_send.at[1], offs_recv.at[src], {"sp": src}).wait_recv()
+            off_rows[1 + src] = offs_in[src].astype(f32) * LOG2E
+
+    def middle_block(g):
+        q_from(3, 2, g).wait_recv()
+        return near_blocks(g, [q_in[1, g]])
+
+    @pl.loop(0, last)
     def _(g):
-        @pl.when(((me == 0) | (me == 3)) & (g % 2 == 0))
-        def _():
-            for u in range(2):
-                near_blocks(g + u, [])
-
         @pl.when(me == 1)
         def _():
+            keys = split_keys(packet[1, g])
+            values = split_values(packet[2, g])
             for i in (1, 0):
-                send(packet.at[0, g], q_in.at[i, g], q_send.at[0, g], q_recv.at[i, g], {"sp": i + 2}).wait_recv()
-            rest = near_blocks(g, [q_in[1, g], q_in[0, g]])
+                q_from(i + 2, 1, g).wait_recv()
             for h in range(2):
+                pieces = attend([q_in[1, g], q_in[0, g]], keys[h], values[h], off_rows[0, pl.ds(2 * g + h, 1), :], False)
                 for i in (1, 0):
-                    res, total = rest[h][1 - i]
+                    res, total = pieces[1 - i]
                     far_r[i, h] = res
                     far_t[i, h] = jnp.exp2(-total)
 
         @pl.when(me == 2)
         def _():
-            send(packet.at[0, g], q_in.at[1, g], q_send.at[0, g], q_recv.at[1, g], {"sp": 3}).wait_recv()
-            rest = near_blocks(g, [q_in[1, g]])
+            rest = middle_block(g)
             for h in range(2):
                 note(2, g, h, *rest[h][0])
             o_out[1, g] = pair(rest[0][0][0], rest[1][0][0]).astype(bf16)
@@ -351,29 +420,16 @@
 
         @pl.when(g == 0)
         def _():
-            convolve(range(step, rows, step))
+            channel_norm()
 
         @pl.when(g == 1)
         def _():
-            convolve_first()
-
-        @pl.when(g == 2)
-        def _():
-            channel_norm()
-
-        @pl.when(g == 3)
-        def _():
             conv_product()
 
         @pl.when(me == 1)
         def _():
-            @pl.when(g == 0)
-            def _():
-                send(offs, offs_in, offs_send, offs_recv, {"sp": 0}).wait_recv()
-                off_rows[1] = offs_in[...].astype(f32) * LOG2E
-
             for t in range(2):
-                send(packet.at[1 + t, g], kv_in.at[t, g], kv_send.at[t, g], kv_recv.at[t, g], {"sp": 0}).wait_recv()
+                kv_from(t, g).wait_recv()
             keys = split_keys(kv_in[0, g])
             values = split_values(kv_in[1, g])
             parts = [[], []]
@@ -392,6 +448,37 @@
             for i in (1, 0):
                 send(o_out.at[i, g], o_in.at[0, g], o_send.at[i, g], o_recv.at[0, g], {"sp": i + 2}).start()
 
+    @pl.when(me == 2)
+    def _():
+        rest = middle_block(last)
+        for h in range(2):
+            res, total = rest[h][0]
+            far_r[1, h] = res
+            far_t[1, h] = jnp.exp2(-total)
+        for src, where in ((1, 0), (0, last)):
+            for t in range(2):
+                send(packet.at[1 + t, last], kv_in.at[t, where], kv_last_send.at[t],
+                     kv_last_recv.at[t, src], {"sp": src}).wait_recv()
+            keys = split_keys(kv_in[0, where])
+            values = split_values(kv_in[1, where])
+            parts = []
+            for h in range(2):
+                (own, own_total), (far, far_total) = attend(
+                    [packet[0, last], q_in[1, last]], keys[h], values[h], off_rows[1 + src, 2 * last + h:2 * last + h + 1, :], False)
+                own = own_r[last, h] + own_t[last, h] * own
+                far = far_r[1, h] + far_t[1, h] * far
+                own_r[last, h] = own
+                if src:
+                    far_r[1, h] = far
+                    own_t[last, h] = own_t[last, h] * jnp.exp2(-own_total)
+                    far_t[1, h] = far_t[1, h] * jnp.exp2(-far_total)
+                else:
+                    note(0, last, h, own, own)
+                    note(2, last, h, far, far)
+                    parts.append(far)
+        o_out[1, last] = pair(*parts).astype(bf16)
+        o_copy(2, 3, last).start()
+
     def stat_rows(which):
         t = jnp.transpose(masses[which])
         return jnp.concatenate([t[0:8], t[HEAD_DIM:HEAD_DIM + 8]], axis=0)
@@ -406,6 +493,18 @@
     def _():
         stat_out[1] = stat_rows(2)
         stat_copy(2, 3).start()
+
+    @pl.when(me == 1)
+    def _():
+        for t in range(2):
+            kv_from(t, last).wait_recv()
+        keys = split_keys(kv_in[0, last])
+        values = split_values(kv_in[1, last])
+        for h in range(2):
+            res, _ = attend([packet[0, last]], keys[h], values[h], off_rows[1, 2 * last + h:2 * last + h + 1, :], False)[0]
+            res = own_r[last, h] + own_t[last, h] * res
+            own_r[last, h] = res
+            note(0, last, h, res, res)
 
     blocks = (lax.broadcasted_iota(jnp.int32, (LANES, LANES), 0) // HEAD_DIM
               == lax.broadcasted_iota(jnp.int32, (LANES, LANES), 1) // HEAD_DIM).astype(bf16)
@@ -432,18 +531,24 @@
 
         @pl.when(me == 2)
         def _():
+            if g == last:
+                close(own)
+            else:
+                through = pair(own_t[g, 0], own_t[g, 1])
+                send(o_out.at[0, g], o_in.at[0, g], o_send.at[0, g], o_recv.at[0, g], {"sp": 1}).wait_recv()
+                close(own + through * o_in[0, g].astype(f32))
+
+        @pl.when(me == 3)
+        def _():
             through = pair(own_t[g, 0], own_t[g, 1])
-            o_copy(1, 2, g).wait_recv()
-            close(own + through * o_in[0, g].astype(f32))
-
-        @pl.when(me == 3)
-        def _():
-            through = pair(own_t[g, 0], own_t[g, 1])
-            tot = far_t[0, 0]
-            middle = jnp.exp2(-pair(tot[:, 12 + g:13 + g], tot[:, 4 + g:5 + g]))
             send(o_out.at[1, g], o_in.at[1, g], o_send.at[1, g], o_recv.at[1, g], {"sp": 2}).wait_recv()
-            send(o_out.at[1, g], o_in.at[0, g], o_send.at[1, g], o_recv.at[0, g], {"sp": 1}).wait_recv()
-            close(own + through * (o_in[1, g].astype(f32) + middle * o_in[0, g].astype(f32)))
+            inner = o_in[1, g].astype(f32)
+            if g < last:
+                tot = far_t[0, 0]
+                middle = jnp.exp2(-pair(tot[:, 12 + g:13 + g], tot[:, 4 + g:5 + g]))
+                send(o_out.at[1, g], o_in.at[0, g], o_send.at[1, g], o_recv.at[0, g], {"sp": 1}).wait_recv()
+                inner = inner + middle * o_in[0, g].astype(f32)
+            close(own + through * inner)
 
     out_copies[1].wait()
     early = groups // 2
@@ -467,6 +572,10 @@
                     out_send.at[c // tile], out_recv.at[c // tile], {"tp": partner})
         copy.start()
         leaves.append(copy)
+    for c in range(0, model, tile):
+        cols = slice(c, c + tile)
+        conv_share[ours, cols] += jnp.dot(
+            heads_ref[ours, cut:], out_weights[1, cut:, cols], preferred_element_type=f32)
 
     mine = stat_rows(0)
 
@@ -493,12 +602,15 @@
         even = mid[8:12] + jnp.exp2(-mid[12:16]) * far[8:12]
         write_log(mine[0:4] + jnp.exp2(-mine[4:8]) * odd, mine[8:12] + jnp.exp2(-mine[12:16]) * even)
 
+    places = [local_copy(log_ref, log_hbm, place_sem.at[0])]
+    places[0].start()
     for c in range(0, model, tile):
         cols = slice(c, c + tile)
-        acc = conv_share[ours, cols] + jnp.dot(
-            heads_ref[ours, cut:], out_weights[1, cut:, cols], preferred_element_type=f32)
         leaves[c // tile].wait()
-        out_ref[:, cols] = (acc + arrived_ref[:, cols].astype(f32)).astype(bf16)
+        out_ref[:, cols] = (conv_share[ours, cols] + arrived_ref[:, cols].astype(f32)).astype(bf16)
+        copy = local_copy(out_ref.at[:, pl.ds(c, tile)], out_hbm.at[:, pl.ds(c, tile)], place_sem.at[1 + c // tile])
+        copy.start()
+        places.append(copy)
 
     @pl.when(me < n - 1)
     def _():
@@ -506,30 +618,40 @@
 
     @pl.when(me == 0)
     def _():
-        offs_copy.wait_send()
-        for g in range(groups):
-            for t in range(2):
+        offs_copy(0, 1).wait_send()
+        offs_copy(0, 2).wait_send()
+        for t in range(2):
+            for g in range(groups):
                 kv_copy(t, g).wait_send()
+            kv_last(t, 0).wait_send()
 
     @pl.when(me == 1)
     def _():
+        offs_copy(1, 2).wait_send()
+        for t in range(2):
+            kv_last(t, 1).wait_send()
         for i in (1, 0):
-            for g in range(groups):
+            for g in range(last):
                 o_copy(1, i + 2, g).wait_send()
             stat_copy(1, i + 2).wait_send()
 
     @pl.when(me == 2)
     def _():
+        for g in range(last):
+            q_copy(2, 1, g).wait_send()
         for g in range(groups):
-            q_copy(2, 1, g).wait_send()
             o_copy(2, 3, g).wait_send()
         stat_copy(2, 3).wait_send()
 
     @pl.when(me == 3)
     def _():
         for g in range(groups):
-            q_copy(3, 1, g).wait_send()
+            if g < last:
+                q_copy(3, 1, g).wait_send()
             q_copy(3, 2, g).wait_send()
+
+    for copy in places:
+        copy.wait()
 
 
 def place(mixed, mass_log, out_ref, log_ref, sem):
@@ -556,7 +678,7 @@
     taps = filter_taps.shape[0]
     model = stream.shape[2]
     share = rows // tp
-    tiles = model // min(512, model)
+    tiles = model // min(1024, model)
 
     vmem = pl.BlockSpec(memory_space=pltpu.VMEM)
     hbm = pl.BlockSpec(memory_space=pl.ANY)
@@ -567,9 +689,17 @@
             jax.ShapeDtypeStruct((share, model), bf16),
             jax.ShapeDtypeStruct((heads, rows), f32),
         ),
-        in_specs=[hbm] + [vmem] * 6 + [hbm] * 7,
-        out_specs=(vmem,) * 2,
+        in_specs=[hbm] * 14,
+        out_specs=(hbm,) * 2,
         scratch_shapes=[
+            pltpu.VMEM((model,), bf16),
+            pltpu.VMEM((heads, rows), bf16),
+            pltpu.VMEM((taps, chans), bf16),
+            pltpu.VMEM((chans,), bf16),
+            pltpu.VMEM((chans,), bf16),
+            pltpu.VMEM((chans,), bf16),
+            pltpu.VMEM((share, model), bf16),
+            pltpu.VMEM((heads, rows), f32),
             pltpu.VMEM((rows, model), bf16),
             pltpu.VMEM((rows, model), bf16),
             pltpu.VMEM((5, model, chans), bf16),
@@ -577,7 +707,7 @@
             pltpu.VMEM((3, groups, rows, LANES), bf16),
             pltpu.VMEM((2, groups, rows, LANES), bf16),
             pltpu.VMEM((2, groups, rows, LANES), bf16),
-            pltpu.VMEM((heads, rows), bf16),
+            pltpu.VMEM((2, heads, rows), bf16),
             pltpu.VMEM((2, groups, rows, LANES), bf16),
             pltpu.VMEM((2, groups, rows, LANES), bf16),
             pltpu.VMEM((2, 16, rows), f32),
@@ -587,7 +717,7 @@
             pltpu.VMEM((2, 2, rows, LANES), f32),
             pltpu.VMEM((2, 2, rows, LANES), f32),
             pltpu.VMEM((3, rows, LANES), f32),
-            pltpu.VMEM((2, heads, rows), f32),
+            pltpu.VMEM((3, heads, rows), f32),
             pltpu.VMEM((slabs, taps + -taps % 8, LANES), f32),
             pltpu.VMEM((rows, heads * HEAD_DIM), bf16),
             pltpu.VMEM((rows, chans), bf16),
@@ -600,7 +730,7 @@
             pltpu.VMEM((slabs, rows, LANES), f32),
             pltpu.VMEM((rows, LANES), f32),
             pltpu.VMEM((rows, LANES), f32),
-            dma, dma((5,)), dma((2,)), dma((2, groups)), dma((2, groups)), dma((2, groups)), dma((2, groups)), dma, dma,
+            dma((6,)), dma((1 + tiles,)), dma((rows // min(64, rows),)), dma((5, chans // (2 * LANES))), dma((2,)), dma((2, groups)), dma((2, groups)), dma((2, groups)), dma((2, groups)), dma((2,)), dma((2, 2)), dma((2,)), dma((2,)),
             dma((2, groups)), dma((2, groups)), dma((2,)), dma((2,)), dma((tiles,)), dma((tiles,)), dma, dma, dma, dma,
         ],
         compiler_params=pltpu.CompilerParams(

time: 32.5 us -> 31.6 us (0.972)
  Pallas kernels: 31.7 us -> 30.8 us
    pallas_call x1, Pallas kernels: 29.8 us -> 28.9 us  [local(): pl.pallas_call(functools.partial(kernel, n, tp, taps, chans * tp), out_sh...]
where the time goes in v3:
time: 31.6 us; the launch traced here: 31.4 us
  Pallas kernels  30.8 us (97%)
  between operations  0.64 us (2%)
    pallas_call x1, Pallas kernels, local(): pl.pallas_call(functools.partial(kernel, n, tp, taps, chans * tp), out_sh...  28.9 us
    pallas_call x1, Pallas kernels, local(): pl.pallas_call(place, out_shape=(jax.ShapeDtypeStruct((share, model), bf1...  1.86 us

profile of v3, /device:TPU:23, one launch (start us, length us, event | category | flops | bytes accessed | tf_op | source)
XLA Modules:
  0.0 31.4 jit_solution(145098525116506572)
XLA Ops:
  0.6 28.9 %shard_map.149 = (bf16[128,2048]{1,0:T(8,128)(2,1)}, f32[8,256]{1,0:T(8,128)}) custom-call(bf16[256,2048]{1,0:T(8,128)(2,1)} %bitcast.8, bf16[2048]{0:T(1024)(128)(2,1)} %ngain_hbm.1, bf16[8,256]{1,0:T(8,128)(2,1)} %bitcast.9, bf16[31,512]{1,0:T(8,128)(2,1)} %taps_hbm.1, bf16[512]{0:T(512)(128)(2,1)} %gain_hbm.1, bf16[512]{0:T(512)(128)(2,1)} %cgain_hbm.1, ...), custom_call_target="tpu_custom_call" | custom-call | tf_op jit(solution)/shard_map/pallas_call | solution.py:686
  29.6 1.9 %shard_map.150 = (bf16[128,2048]{1,0:T(8,128)(2,1)}, f32[8,256]{1,0:T(8,128)}) custom-call(bf16[128,2048]{1,0:T(8,128)(2,1)} %get-tuple-element.6.mixed, f32[8,256]{1,0:T(8,128)} %get-tuple-element.7.mass_log), custom_call_target="tpu_custom_call" | custom-call | tf_op jit(solution)/shard_map/pallas_call | solution.py:740

commit v4 on v3

--- a/solution.py
+++ b/solution.py
@@ -22,12 +22,12 @@
     n, tp, taps, total_channels,
     stream_hbm, ngain_hbm, offs_hbm, taps_hbm, gain_hbm, cgain_hbm, cshift_hbm,
     q_hbm, k_hbm, v_hbm, in_hbm, gate_hbm, attend_hbm, filter_hbm,
-    out_hbm, log_hbm,
-    ngain, offs, raw_taps, gain_ref, cgain_ref, cshift_ref, out_ref, log_ref,
+    out_ref, log_ref,
+    ngain, offs, raw_taps, gain_ref, cgain_ref, cshift_ref,
     stream, normed, weights, out_weights, packet, q_in, kv_in, offs_in, o_out, o_in, stat_out, stat_in,
     own_r, own_t, far_r, far_t, masses, off_rows, tap_ref, heads_ref, conv_ref, conv_share, leaving, arrived_ref,
     gated, halo, ext, filt, stats, stats_got,
-    small_sem, place_sem, stream_sem, weight_sem, out_weight_sem, q_send, q_recv, kv_send, kv_recv, kv_last_send, kv_last_recv, offs_send, offs_recv,
+    small_sem, stream_sem, weight_sem, out_weight_sem, q_send, q_recv, kv_send, kv_recv, kv_last_send, kv_last_recv, offs_send, offs_recv,
     o_send, o_recv, stat_send, stat_recv, out_send, out_recv, halo_send, halo_recv, chan_send, chan_recv,
 ):
     f32, bf16 = jnp.float32, jnp.bfloat16
@@ -121,22 +121,18 @@
     for copy in small[1:]:
         copy.wait()
 
-    for d in range(n):
-        @pl.when(me == d)
-        def _(d=d):
-            pl.semaphore_wait(barrier, len(peers[d]) + tp - 1)
-
     def q_copy(src_dev, dst_dev, g):
         return send(packet.at[0, g], q_in.at[src_dev - 2, g], q_send.at[dst_dev - 1, g],
                     q_recv.at[src_dev - 2, g], {"sp": dst_dev})
 
-    last = groups - 1
+    far_g = 0
+    dev1_groups = range(1, groups)
 
     def kv_copy(t, g):
         return send(packet.at[1 + t, g], kv_in.at[t, g], kv_send.at[t, g], kv_recv.at[t, g], {"sp": 1})
 
     def kv_last(t, src_dev):
-        return send(packet.at[1 + t, last], kv_in.at[t, 0 if src_dev else last],
+        return send(packet.at[1 + t, far_g], kv_in.at[t, src_dev],
                     kv_last_send.at[t], kv_last_recv.at[t, src_dev], {"sp": 2})
 
     def offs_copy(src_dev, dst_dev):
@@ -149,15 +145,6 @@
     def stat_copy(src_dev, dst_dev):
         return send(stat_out.at[dst_dev - 2], stat_in.at[src_dev - 1], stat_send.at[dst_dev - 2],
                     stat_recv.at[src_dev - 1], {"sp": dst_dev})
-
-    @pl.when(me == 0)
-    def _():
-        offs_copy(0, 1).start()
-        offs_copy(0, 2).start()
-
-    @pl.when(me == 1)
-    def _():
-        offs_copy(1, 2).start()
 
     def keep(slot, half, y):
         factor = jnp.where(slot == 0, LOG2E * HEAD_DIM ** (-0.5), 1.0).astype(f32)
@@ -177,28 +164,37 @@
     for half in range(halves):
         project([(0, half), (1, half)])
 
+        if half == 0:
+            for d in range(n):
+                @pl.when(me == d)
+                def _(d=d):
+                    pl.semaphore_wait(barrier, len(peers[d]) + tp - 1)
+
         @pl.when(me == 0)
         def _():
             if half == 0:
-                kv_copy(0, 0).start()
-                kv_copy(1, 0).start()
+                for t in range(2):
+                    kv_last(t, 0).start()
+                offs_copy(0, 1).start()
+                offs_copy(0, 2).start()
+
+        @pl.when(me == 1)
+        def _():
+            if half == 0:
+                offs_copy(1, 2).start()
 
         @pl.when(me == 2)
         def _():
             for g in (2 * half, 2 * half + 1):
-                if g < last:
+                if g in dev1_groups:
                     q_copy(2, 1, g).start()
 
         @pl.when(me == 3)
         def _():
-            if half > 0:
-                q_copy(3, 2, 2 * half - 1).start()
-            q_copy(3, 1, 2 * half).start()
-            q_copy(3, 2, 2 * half).start()
-            if 2 * half + 1 < last:
-                q_copy(3, 1, 2 * half + 1).start()
-            else:
-                q_copy(3, 2, 2 * half + 1).start()
+            for g in (2 * half, 2 * half + 1):
+                if g in dev1_groups:
+                    q_copy(3, 1, g).start()
+                q_copy(3, 2, g).start()
 
     for copy in out_copies:
         copy.start()
@@ -230,13 +226,9 @@
 
     @pl.when(me == 0)
     def _():
-        for g in range(1, last):
+        for g in (*dev1_groups, far_g):
             for t in range(2):
                 kv_copy(t, g).start()
-        for t in range(2):
-            kv_last(t, 0).start()
-        for t in range(2):
-            kv_copy(t, last).start()
 
     project([(2, half) for half in range(halves)])
 
@@ -370,8 +362,6 @@
             for u in range(2):
                 near_blocks(2 * half + u, [])
 
-    convolve_first()
-
     def q_from(src_dev, dst_dev, g):
         return send(packet.at[0, g], q_in.at[src_dev - 2, g], q_send.at[dst_dev - 1, g],
                     q_recv.at[src_dev - 2, g], {"sp": src_dev})
@@ -379,6 +369,20 @@
     def kv_from(t, g):
         return send(packet.at[1 + t, g], kv_in.at[t, g], kv_send.at[t, g], kv_recv.at[t, g], {"sp": 0})
 
+    def middle_block(g):
+        q_from(3, 2, g).wait_recv()
+        return near_blocks(g, [q_in[1, g]])
+
+    @pl.when(me == 2)
+    def _():
+        rest = middle_block(far_g)
+        for h in range(2):
+            res, total = rest[h][0]
+            far_r[1, h] = res
+            far_t[1, h] = jnp.exp2(-total)
+
+    convolve_first()
+
     @pl.when(me == 1)
     def _():
         offs_copy_back = send(offs, offs_in.at[0], offs_send.at[0], offs_recv.at[0], {"sp": 0})
@@ -391,11 +395,34 @@
             send(offs, offs_in.at[src], offs_send.at[1], offs_recv.at[src], {"sp": src}).wait_recv()
             off_rows[1 + src] = offs_in[src].astype(f32) * LOG2E
 
-    def middle_block(g):
-        q_from(3, 2, g).wait_recv()
-        return near_blocks(g, [q_in[1, g]])
-
-    @pl.loop(0, last)
+    def far_blocks():
+        @pl.when(me == 2)
+        def _():
+            for src in (1, 0):
+                for t in range(2):
+                    send(packet.at[1 + t, far_g], kv_in.at[t, src], kv_last_send.at[t],
+                         kv_last_recv.at[t, src], {"sp": src}).wait_recv()
+                keys = split_keys(kv_in[0, src])
+                values = split_values(kv_in[1, src])
+                parts = []
+                for h in range(2):
+                    (own, own_total), (far, far_total) = attend(
+                        [packet[0, far_g], q_in[1, far_g]], keys[h], values[h], off_rows[1 + src, 2 * far_g + h:2 * far_g + h + 1, :], False)
+                    own = own_r[far_g, h] + own_t[far_g, h] * own
+                    far = far_r[1, h] + far_t[1, h] * far
+                    own_r[far_g, h] = own
+                    if src:
+                        far_r[1, h] = far
+                        own_t[far_g, h] = own_t[far_g, h] * jnp.exp2(-own_total)
+                        far_t[1, h] = far_t[1, h] * jnp.exp2(-far_total)
+                    else:
+                        note(0, far_g, h, own, own)
+                        note(2, far_g, h, far, far)
+                        parts.append(far)
+            o_out[1, far_g] = pair(*parts).astype(bf16)
+            o_copy(2, 3, far_g).start()
+
+    @pl.loop(1, groups)
     def _(g):
         @pl.when(me == 1)
         def _():
@@ -418,11 +445,12 @@
             o_out[1, g] = pair(rest[0][0][0], rest[1][0][0]).astype(bf16)
             send(o_out.at[1, g], o_in.at[1, g], o_send.at[1, g], o_recv.at[1, g], {"sp": 3}).start()
 
-        @pl.when(g == 0)
+        @pl.when(g == 1)
         def _():
             channel_norm()
-
-        @pl.when(g == 1)
+            far_blocks()
+
+        @pl.when(g == 2)
         def _():
             conv_product()
 
@@ -448,37 +476,6 @@
             for i in (1, 0):
                 send(o_out.at[i, g], o_in.at[0, g], o_send.at[i, g], o_recv.at[0, g], {"sp": i + 2}).start()
 
-    @pl.when(me == 2)
-    def _():
-        rest = middle_block(last)
-        for h in range(2):
-            res, total = rest[h][0]
-            far_r[1, h] = res
-            far_t[1, h] = jnp.exp2(-total)
-        for src, where in ((1, 0), (0, last)):
-            for t in range(2):
-                send(packet.at[1 + t, last], kv_in.at[t, where], kv_last_send.at[t],
-                     kv_last_recv.at[t, src], {"sp": src}).wait_recv()
-            keys = split_keys(kv_in[0, where])
-            values = split_values(kv_in[1, where])
-            parts = []
-            for h in range(2):
-                (own, own_total), (far, far_total) = attend(
-                    [packet[0, last], q_in[1, last]], keys[h], values[h], off_rows[1 + src, 2 * last + h:2 * last + h + 1, :], False)
-                own = own_r[last, h] + own_t[last, h] * own
-                far = far_r[1, h] + far_t[1, h] * far
-                own_r[last, h] = own
-                if src:
-                    far_r[1, h] = far
-                    own_t[last, h] = own_t[last, h] * jnp.exp2(-own_total)
-                    far_t[1, h] = far_t[1, h] * jnp.exp2(-far_total)
-                else:
-                    note(0, last, h, own, own)
-                    note(2, last, h, far, far)
-                    parts.append(far)
-        o_out[1, last] = pair(*parts).astype(bf16)
-        o_copy(2, 3, last).start()
-
     def stat_rows(which):
         t = jnp.transpose(masses[which])
         return jnp.concatenate([t[0:8], t[HEAD_DIM:HEAD_DIM + 8]], axis=0)
@@ -497,14 +494,14 @@
     @pl.when(me == 1)
     def _():
         for t in range(2):
-            kv_from(t, last).wait_recv()
-        keys = split_keys(kv_in[0, last])
-        values = split_values(kv_in[1, last])
+            kv_from(t, far_g).wait_recv()
+        keys = split_keys(kv_in[0, far_g])
+        values = split_values(kv_in[1, far_g])
         for h in range(2):
-            res, _ = attend([packet[0, last]], keys[h], values[h], off_rows[1, 2 * last + h:2 * last + h + 1, :], False)[0]
-            res = own_r[last, h] + own_t[last, h] * res
-            own_r[last, h] = res
-            note(0, last, h, res, res)
+            res, _ = attend([packet[0, far_g]], keys[h], values[h], off_rows[1, 2 * far_g + h:2 * far_g + h + 1, :], False)[0]
+            res = own_r[far_g, h] + own_t[far_g, h] * res
+            own_r[far_g, h] = res
+            note(0, far_g, h, res, res)
 
     blocks = (lax.broadcasted_iota(jnp.int32, (LANES, LANES), 0) // HEAD_DIM
               == lax.broadcasted_iota(jnp.int32, (LANES, LANES), 1) // HEAD_DIM).astype(bf16)
@@ -531,7 +528,7 @@
 
         @pl.when(me == 2)
         def _():
-            if g == last:
+            if g == far_g:
                 close(own)
             else:
                 through = pair(own_t[g, 0], own_t[g, 1])
@@ -543,7 +540,7 @@
             through = pair(own_t[g, 0], own_t[g, 1])
             send(o_out.at[1, g], o_in.at[1, g], o_send.at[1, g], o_recv.at[1, g], {"sp": 2}).wait_recv()
             inner = o_in[1, g].astype(f32)
-            if g < last:
+            if g != far_g:
                 tot = far_t[0, 0]
                 middle = jnp.exp2(-pair(tot[:, 12 + g:13 + g], tot[:, 4 + g:5 + g]))
                 send(o_out.at[1, g], o_in.at[0, g], o_send.at[1, g], o_recv.at[0, g], {"sp": 1}).wait_recv()
@@ -602,15 +599,10 @@
         even = mid[8:12] + jnp.exp2(-mid[12:16]) * far[8:12]
         write_log(mine[0:4] + jnp.exp2(-mine[4:8]) * odd, mine[8:12] + jnp.exp2(-mine[12:16]) * even)
 
-    places = [local_copy(log_ref, log_hbm, place_sem.at[0])]
-    places[0].start()
     for c in range(0, model, tile):
         cols = slice(c, c + tile)
         leaves[c // tile].wait()
         out_ref[:, cols] = (conv_share[ours, cols] + arrived_ref[:, cols].astype(f32)).astype(bf16)
-        copy = local_copy(out_ref.at[:, pl.ds(c, tile)], out_hbm.at[:, pl.ds(c, tile)], place_sem.at[1 + c // tile])
-        copy.start()
-        places.append(copy)
 
     @pl.when(me < n - 1)
     def _():
@@ -631,13 +623,13 @@
         for t in range(2):
             kv_last(t, 1).wait_send()
         for i in (1, 0):
-            for g in range(last):
+            for g in dev1_groups:
                 o_copy(1, i + 2, g).wait_send()
             stat_copy(1, i + 2).wait_send()
 
     @pl.when(me == 2)
     def _():
-        for g in range(last):
+        for g in dev1_groups:
             q_copy(2, 1, g).wait_send()
         for g in range(groups):
             o_copy(2, 3, g).wait_send()
@@ -646,12 +638,9 @@
     @pl.when(me == 3)
     def _():
         for g in range(groups):
-            if g < last:
+            if g in dev1_groups:
                 q_copy(3, 1, g).wait_send()
             q_copy(3, 2, g).wait_send()
-
-    for copy in places:
-        copy.wait()
 
 
 def place(mixed, mass_log, out_ref, log_ref, sem):
@@ -681,16 +670,13 @@
     tiles = model // min(1024, model)
 
     vmem = pl.BlockSpec(memory_space=pltpu.VMEM)
-    hbm = pl.BlockSpec(memory_space=pl.ANY)
+    hbm = pl.BlockSpec(memory_space=pltpu.HBM)
     dma = pltpu.SemaphoreType.DMA
     mixed, mass_log = pl.pallas_call(
         functools.partial(kernel, n, tp, taps, chans * tp),
-        out_shape=(
-            jax.ShapeDtypeStruct((share, model), bf16),
-            jax.ShapeDtypeStruct((heads, rows), f32),
-        ),
+        out_shape=(pltpu.VMEM((share, model), bf16), pltpu.VMEM((heads, rows), f32)),
         in_specs=[hbm] * 14,
-        out_specs=(hbm,) * 2,
+        out_specs=(vmem,) * 2,
         scratch_shapes=[
             pltpu.VMEM((model,), bf16),
             pltpu.VMEM((heads, rows), bf16),
@@ -698,8 +684,6 @@
             pltpu.VMEM((chans,), bf16),
             pltpu.VMEM((chans,), bf16),
             pltpu.VMEM((chans,), bf16),
-            pltpu.VMEM((share, model), bf16),
-            pltpu.VMEM((heads, rows), f32),
             pltpu.VMEM((rows, model), bf16),
             pltpu.VMEM((rows, model), bf16),
             pltpu.VMEM((5, model, chans), bf16),
@@ -730,7 +714,7 @@
             pltpu.VMEM((slabs, rows, LANES), f32),
             pltpu.VMEM((rows, LANES), f32),
             pltpu.VMEM((rows, LANES), f32),
-            dma((6,)), dma((1 + tiles,)), dma((rows // min(64, rows),)), dma((5, chans // (2 * LANES))), dma((2,)), dma((2, groups)), dma((2, groups)), dma((2, groups)), dma((2, groups)), dma((2,)), dma((2, 2)), dma((2,)), dma((2,)),
+            dma((6,)), dma((rows // min(64, rows),)), dma((5, chans // (2 * LANES))), dma((2,)), dma((2, groups)), dma((2, groups)), dma((2, groups)), dma((2, groups)), dma((2,)), dma((2, 2)), dma((2,)), dma((2,)),
             dma((2, groups)), dma((2, groups)), dma((2,)), dma((2,)), dma((tiles,)), dma((tiles,)), dma, dma, dma, dma,
         ],
         compiler_params=pltpu.CompilerParams(
@@ -746,7 +730,7 @@
         in_specs=[vmem] * 2,
         out_specs=(hbm,) * 2,
         scratch_shapes=[dma((2,))],
-    )(mixed, mass_log)
+    )(*[pltpu.with_memory_space_constraint(a, pltpu.VMEM) for a in (mixed, mass_log)])
     return (mixed[None], mass_log.T[None])
 
 

time: 31.6 us -> 29.3 us (0.927)
  the two profiles are of different devices: /device:TPU:23 before, /device:TPU:27 now
where the time goes in v4:
time: 29.3 us; the launch traced here: 29.2 us
  Pallas kernels  28.5 us (97%)
  between operations  0.64 us (2%)
    pallas_call x1, Pallas kernels, local(): pl.pallas_call(functools.partial(kernel, n, tp, taps, chans * tp), out_sh...  27.7 us
    pallas_call x1, Pallas kernels, local(): pl.pallas_call(place, out_shape=(jax.ShapeDtypeStruct((share, model), bf1...  0.81 us

profile of v4, /device:TPU:27, one launch (start us, length us, event | category | flops | bytes accessed | tf_op | source)
XLA Modules:
  0.0 29.2 jit_solution(6653968351728655720)
XLA Ops:
  0.6 27.7 %shard_map.149 = (bf16[128,2048]{1,0:T(8,128)(2,1)S(1)}, f32[8,256]{1,0:T(8,128)S(1)}) custom-call(bf16[256,2048]{1,0:T(8,128)(2,1)} %bitcast.8, bf16[2048]{0:T(1024)(128)(2,1)} %ngain_hbm.1, bf16[8,256]{1,0:T(8,128)(2,1)} %bitcast.9, bf16[31,512]{1,0:T(8,128)(2,1)} %taps_hbm.1, bf16[512]{0:T(512)(128)(2,1)} %gain_hbm.1, bf16[512]{0:T(512)(128)(2,1)} %cgain_hbm.1, ...), custom_call_target="tpu_custom_call" | custom-call | tf_op jit(solution)/shard_map/pallas_call | solution.py:675
  28.4 0.8 %shard_map.150 = (bf16[128,2048]{1,0:T(8,128)(2,1)}, f32[8,256]{1,0:T(8,128)}) custom-call(bf16[128,2048]{1,0:T(8,128)(2,1)S(1)} %get-tuple-element.6.mixed, f32[8,256]{1,0:T(8,128)S(1)} %get-tuple-element.7.mass_log), custom_call_target="tpu_custom_call" | custom-call | tf_op jit(solution)/shard_map/pallas_call | solution.py:724

commit v5 on v4

--- a/solution.py
+++ b/solution.py
@@ -28,7 +28,7 @@
     own_r, own_t, far_r, far_t, masses, off_rows, tap_ref, heads_ref, conv_ref, conv_share, leaving, arrived_ref,
     gated, halo, ext, filt, stats, stats_got,
     small_sem, stream_sem, weight_sem, out_weight_sem, q_send, q_recv, kv_send, kv_recv, kv_last_send, kv_last_recv, offs_send, offs_recv,
-    o_send, o_recv, stat_send, stat_recv, out_send, out_recv, halo_send, halo_recv, chan_send, chan_recv,
+    o_send, o_recv, stat_send, stat_recv, out_send, out_recv, halo_send, halo_recv, chan_send, chan_recv, entered,
 ):
     f32, bf16 = jnp.float32, jnp.bfloat16
     me = lax.axis_index("sp")
@@ -88,7 +88,7 @@
         copy.start()
 
     barrier = pltpu.get_barrier_semaphore()
-    peers = {0: (1, 2), 1: (0, 2, 3), 2: (0, 1, 3), 3: (1, 2)}
+    peers = {0: (1,), 1: (0, 2, 3), 2: (1, 3), 3: (1, 2)}
     pl.semaphore_signal(barrier, inc=1, device_id={"tp": partner}, device_id_type=MESH)
     for d in range(n):
         @pl.when(me == d)
@@ -128,8 +128,8 @@
     far_g = 0
     dev1_groups = range(1, groups)
 
-    def kv_copy(t, g):
-        return send(packet.at[1 + t, g], kv_in.at[t, g], kv_send.at[t, g], kv_recv.at[t, g], {"sp": 1})
+    def kv_copy(src_dev, t, g):
+        return send(packet.at[1 + t, g], kv_in.at[t, g], kv_send.at[t, g], kv_recv.at[t, g], {"sp": src_dev + 1})
 
     def kv_last(t, src_dev):
         return send(packet.at[1 + t, far_g], kv_in.at[t, src_dev],
@@ -170,31 +170,35 @@
                 def _(d=d):
                     pl.semaphore_wait(barrier, len(peers[d]) + tp - 1)
 
+        groups_here = (2 * half, 2 * half + 1)
+
         @pl.when(me == 0)
         def _():
             if half == 0:
+                offs_copy(0, 1).start()
                 for t in range(2):
-                    kv_last(t, 0).start()
-                offs_copy(0, 1).start()
-                offs_copy(0, 2).start()
+                    kv_copy(0, t, 1).start()
 
         @pl.when(me == 1)
         def _():
             if half == 0:
+                pl.semaphore_signal(entered, inc=1, device_id={"sp": 0}, device_id_type=MESH)
                 offs_copy(1, 2).start()
 
         @pl.when(me == 2)
         def _():
-            for g in (2 * half, 2 * half + 1):
+            if half == 0:
+                offs_copy(2, 3).start()
+            q_copy(2, 1, 1 + half).start()
+            for g in groups_here:
                 if g in dev1_groups:
-                    q_copy(2, 1, g).start()
+                    kv_copy(2, 0, g).start()
 
         @pl.when(me == 3)
         def _():
-            for g in (2 * half, 2 * half + 1):
-                if g in dev1_groups:
-                    q_copy(3, 1, g).start()
-                q_copy(3, 2, g).start()
+            q_copy(3, 1, 1 + half).start()
+            if half == 1:
+                q_copy(3, 2, far_g).start()
 
     for copy in out_copies:
         copy.start()
@@ -220,15 +224,30 @@
 
     halo_copy = send(gated, halo, halo_send, halo_recv, {"sp": lax.rem(me + 1, n)})
 
+    @pl.when(me == 0)
+    def _():
+        pl.semaphore_wait(entered, 1)
+        offs_copy(0, 2).start()
+        for t in range(2):
+            kv_last(t, 0).start()
+        for g in dev1_groups[1:]:
+            for t in range(2):
+                kv_copy(0, t, g).start()
+
+    for d in (2, 3):
+        @pl.when(me == d)
+        def _(d=d):
+            for g in dev1_groups[2:]:
+                q_copy(d, 1, g).start()
+
     @pl.when(me < n - 1)
     def _():
         halo_copy.start()
 
     @pl.when(me == 0)
     def _():
-        for g in (*dev1_groups, far_g):
-            for t in range(2):
-                kv_copy(t, g).start()
+        for t in range(2):
+            kv_copy(0, t, far_g).start()
 
     project([(2, half) for half in range(halves)])
 
@@ -236,6 +255,11 @@
     def _():
         for t in range(2):
             kv_last(t, 1).start()
+
+    @pl.when(me == 2)
+    def _():
+        for g in dev1_groups:
+            kv_copy(2, 1, g).start()
 
     step = min(128, rows)
 
@@ -355,115 +379,52 @@
 
     convolve(range(step, rows, step))
 
-    @pl.when(me != 2)
+    def q_from(src_dev, dst_dev, g):
+        return send(packet.at[0, g], q_in.at[src_dev - 2, g], q_send.at[dst_dev - 1, g],
+                    q_recv.at[src_dev - 2, g], {"sp": src_dev})
+
+    def kv_from(src_dev, g):
+        for t in range(2):
+            send(packet.at[1 + t, g], kv_in.at[t, g], kv_send.at[t, g], kv_recv.at[t, g], {"sp": src_dev}).wait_recv()
+        return split_keys(kv_in[0, g]), split_values(kv_in[1, g])
+
+    def offs_from(src_dev, dst_dev, row):
+        send(offs, offs_in.at[src_dev], offs_send.at[dst_dev - 1], offs_recv.at[src_dev], {"sp": src_dev}).wait_recv()
+        off_rows[row] = offs_in[src_dev].astype(f32) * LOG2E
+
+    def off_of(row, g, h):
+        return off_rows[row, pl.ds(2 * g + h, 1), :]
+
+    def stat_rows(which):
+        t = jnp.transpose(masses[which])
+        return jnp.concatenate([t[0:8], t[HEAD_DIM:HEAD_DIM + 8]], axis=0)
+
+    @pl.when((me == 0) | (me == 3))
     def _():
         @pl.loop(0, groups // 2)
         def _(half):
             for u in range(2):
                 near_blocks(2 * half + u, [])
 
-    def q_from(src_dev, dst_dev, g):
-        return send(packet.at[0, g], q_in.at[src_dev - 2, g], q_send.at[dst_dev - 1, g],
-                    q_recv.at[src_dev - 2, g], {"sp": src_dev})
-
-    def kv_from(t, g):
-        return send(packet.at[1 + t, g], kv_in.at[t, g], kv_send.at[t, g], kv_recv.at[t, g], {"sp": 0})
-
-    def middle_block(g):
-        q_from(3, 2, g).wait_recv()
-        return near_blocks(g, [q_in[1, g]])
-
-    @pl.when(me == 2)
-    def _():
-        rest = middle_block(far_g)
-        for h in range(2):
-            res, total = rest[h][0]
-            far_r[1, h] = res
-            far_t[1, h] = jnp.exp2(-total)
-
-    convolve_first()
-
     @pl.when(me == 1)
     def _():
-        offs_copy_back = send(offs, offs_in.at[0], offs_send.at[0], offs_recv.at[0], {"sp": 0})
-        offs_copy_back.wait_recv()
-        off_rows[1] = offs_in[0].astype(f32) * LOG2E
-
-    @pl.when(me == 2)
-    def _():
-        for src in range(2):
-            send(offs, offs_in.at[src], offs_send.at[1], offs_recv.at[src], {"sp": src}).wait_recv()
-            off_rows[1 + src] = offs_in[src].astype(f32) * LOG2E
-
-    def far_blocks():
-        @pl.when(me == 2)
-        def _():
-            for src in (1, 0):
-                for t in range(2):
-                    send(packet.at[1 + t, far_g], kv_in.at[t, src], kv_last_send.at[t],
-                         kv_last_recv.at[t, src], {"sp": src}).wait_recv()
-                keys = split_keys(kv_in[0, src])
-                values = split_values(kv_in[1, src])
-                parts = []
-                for h in range(2):
-                    (own, own_total), (far, far_total) = attend(
-                        [packet[0, far_g], q_in[1, far_g]], keys[h], values[h], off_rows[1 + src, 2 * far_g + h:2 * far_g + h + 1, :], False)
-                    own = own_r[far_g, h] + own_t[far_g, h] * own
-                    far = far_r[1, h] + far_t[1, h] * far
-                    own_r[far_g, h] = own
-                    if src:
-                        far_r[1, h] = far
-                        own_t[far_g, h] = own_t[far_g, h] * jnp.exp2(-own_total)
-                        far_t[1, h] = far_t[1, h] * jnp.exp2(-far_total)
-                    else:
-                        note(0, far_g, h, own, own)
-                        note(2, far_g, h, far, far)
-                        parts.append(far)
-            o_out[1, far_g] = pair(*parts).astype(bf16)
-            o_copy(2, 3, far_g).start()
-
-    @pl.loop(1, groups)
-    def _(g):
-        @pl.when(me == 1)
-        def _():
-            keys = split_keys(packet[1, g])
-            values = split_values(packet[2, g])
+        near_blocks(far_g, [])
+        offs_from(0, 1, 1)
+
+        @pl.loop(1, groups)
+        def _(g):
             for i in (1, 0):
                 q_from(i + 2, 1, g).wait_recv()
+            rest = near_blocks(g, [q_in[1, g], q_in[0, g]])
             for h in range(2):
-                pieces = attend([q_in[1, g], q_in[0, g]], keys[h], values[h], off_rows[0, pl.ds(2 * g + h, 1), :], False)
                 for i in (1, 0):
-                    res, total = pieces[1 - i]
+                    res, total = rest[h][1 - i]
                     far_r[i, h] = res
                     far_t[i, h] = jnp.exp2(-total)
-
-        @pl.when(me == 2)
-        def _():
-            rest = middle_block(g)
-            for h in range(2):
-                note(2, g, h, *rest[h][0])
-            o_out[1, g] = pair(rest[0][0][0], rest[1][0][0]).astype(bf16)
-            send(o_out.at[1, g], o_in.at[1, g], o_send.at[1, g], o_recv.at[1, g], {"sp": 3}).start()
-
-        @pl.when(g == 1)
-        def _():
-            channel_norm()
-            far_blocks()
-
-        @pl.when(g == 2)
-        def _():
-            conv_product()
-
-        @pl.when(me == 1)
-        def _():
-            for t in range(2):
-                kv_from(t, g).wait_recv()
-            keys = split_keys(kv_in[0, g])
-            values = split_values(kv_in[1, g])
+            keys, values = kv_from(0, g)
             parts = [[], []]
             for h in range(2):
-                pieces = attend([q_in[1, g], q_in[0, g], packet[0, g]], keys[h], values[h],
-                                off_rows[1, pl.ds(2 * g + h, 1), :], False)
+                pieces = attend([q_in[1, g], q_in[0, g], packet[0, g]], keys[h], values[h], off_of(1, g, h), False)
                 for i in (1, 0):
                     res = far_r[i, h] + far_t[i, h] * pieces[1 - i][0]
                     note(1 + i, g, h, res, res)
@@ -476,41 +437,86 @@
             for i in (1, 0):
                 send(o_out.at[i, g], o_in.at[0, g], o_send.at[i, g], o_recv.at[0, g], {"sp": i + 2}).start()
 
-    def stat_rows(which):
-        t = jnp.transpose(masses[which])
-        return jnp.concatenate([t[0:8], t[HEAD_DIM:HEAD_DIM + 8]], axis=0)
-
-    @pl.when(me == 1)
-    def _():
         for i in (1, 0):
             stat_out[i] = stat_rows(1 + i)
             stat_copy(1, i + 2).start()
 
     @pl.when(me == 2)
     def _():
+        near_blocks(1, [])
+
+        @pl.loop(1, 2)
+        def _(half):
+            for u in range(2):
+                near_blocks(2 * half + u, [])
+
+    convolve_first()
+
+    @pl.when(me == 2)
+    def _():
+        q_from(3, 2, far_g).wait_recv()
+        rest = near_blocks(far_g, [q_in[1, far_g]])
+        for h in range(2):
+            res, total = rest[h][0]
+            far_r[1, h] = res
+            far_t[1, h] = jnp.exp2(-total)
+        offs_from(1, 2, 2)
+        offs_from(0, 2, 1)
+        for src in (1, 0):
+            for t in range(2):
+                send(packet.at[1 + t, far_g], kv_in.at[t, src], kv_last_send.at[t],
+                     kv_last_recv.at[t, src], {"sp": src}).wait_recv()
+            keys = split_keys(kv_in[0, src])
+            values = split_values(kv_in[1, src])
+            parts = []
+            for h in range(2):
+                (own, own_total), (far, far_total) = attend(
+                    [packet[0, far_g], q_in[1, far_g]], keys[h], values[h], off_rows[1 + src, 2 * far_g + h:2 * far_g + h + 1, :], False)
+                own = own_r[far_g, h] + own_t[far_g, h] * own
+                far = far_r[1, h] + far_t[1, h] * far
+                own_r[far_g, h] = own
+                if src:
+                    far_r[1, h] = far
+                    own_t[far_g, h] = own_t[far_g, h] * jnp.exp2(-own_total)
+                    far_t[1, h] = far_t[1, h] * jnp.exp2(-far_total)
+                else:
+                    note(0, far_g, h, own, own)
+                    note(2, far_g, h, far, far)
+                    parts.append(far)
+        o_out[1, far_g] = pair(*parts).astype(bf16)
+        o_out[1, far_g] = pair(*parts).astype(bf16)
+        o_copy(2, 3, far_g).start()
         stat_out[1] = stat_rows(2)
         stat_copy(2, 3).start()
 
+    channel_norm()
+    conv_product()
+
     @pl.when(me == 1)
     def _():
-        for t in range(2):
-            kv_from(t, far_g).wait_recv()
-        keys = split_keys(kv_in[0, far_g])
-        values = split_values(kv_in[1, far_g])
+        keys, values = kv_from(0, far_g)
         for h in range(2):
-            res, _ = attend([packet[0, far_g]], keys[h], values[h], off_rows[1, 2 * far_g + h:2 * far_g + h + 1, :], False)[0]
+            res, _ = attend([packet[0, far_g]], keys[h], values[h], off_of(1, far_g, h), False)[0]
             res = own_r[far_g, h] + own_t[far_g, h] * res
             own_r[far_g, h] = res
             note(0, far_g, h, res, res)
 
+    @pl.when(me == 3)
+    def _():
+        offs_from(2, 3, 1)
+        for g in dev1_groups:
+            keys, values = kv_from(2, g)
+            for h in range(2):
+                res, total = attend([packet[0, g]], keys[h], values[h], off_of(1, g, h), False)[0]
+                through = own_t[g, h]
+                res = own_r[g, h] + through * res
+                own_r[g, h] = res
+                own_t[g, h] = through * jnp.exp2(-total)
+                near = masses[0][:, (HEAD_DIM, 0)[h] + 4 + g:(HEAD_DIM, 0)[h] + 5 + g]
+                note(0, g, h, res, total + near)
+
     blocks = (lax.broadcasted_iota(jnp.int32, (LANES, LANES), 0) // HEAD_DIM
               == lax.broadcasted_iota(jnp.int32, (LANES, LANES), 1) // HEAD_DIM).astype(bf16)
-
-    @pl.when(me == 3)
-    def _():
-        stat_copy(2, 3).wait_recv()
-        rest = jnp.zeros((LANES - 16, rows), f32)
-        far_t[0, 0] = jnp.transpose(jnp.concatenate([stat_in[1], rest], axis=0))
 
     def finish(g):
         cols = slice(g * LANES, (g + 1) * LANES)
@@ -538,14 +544,9 @@
         @pl.when(me == 3)
         def _():
             through = pair(own_t[g, 0], own_t[g, 1])
-            send(o_out.at[1, g], o_in.at[1, g], o_send.at[1, g], o_recv.at[1, g], {"sp": 2}).wait_recv()
-            inner = o_in[1, g].astype(f32)
-            if g != far_g:
-                tot = far_t[0, 0]
-                middle = jnp.exp2(-pair(tot[:, 12 + g:13 + g], tot[:, 4 + g:5 + g]))
-                send(o_out.at[1, g], o_in.at[0, g], o_send.at[1, g], o_recv.at[0, g], {"sp": 1}).wait_recv()
-                inner = inner + middle * o_in[0, g].astype(f32)
-            close(own + through * inner)
+            src = 2 if g == far_g else 1
+            send(o_out.at[1, g], o_in.at[src - 1, g], o_send.at[1, g], o_recv.at[src - 1, g], {"sp": src}).wait_recv()
+            close(own + through * o_in[src - 1, g].astype(f32))
 
     out_copies[1].wait()
     early = groups // 2
@@ -593,11 +594,10 @@
 
     @pl.when(me == 3)
     def _():
-        send(stat_out.at[1], stat_in.at[0], stat_send.at[1], stat_recv.at[0], {"sp": 1}).wait_recv()
-        far, mid = stat_in[0], stat_in[1]
-        odd = mid[0:4] + jnp.exp2(-mid[4:8]) * far[0:4]
-        even = mid[8:12] + jnp.exp2(-mid[12:16]) * far[8:12]
-        write_log(mine[0:4] + jnp.exp2(-mine[4:8]) * odd, mine[8:12] + jnp.exp2(-mine[12:16]) * even)
+        for src in (1, 2):
+            send(stat_out.at[1], stat_in.at[src - 1], stat_send.at[1], stat_recv.at[src - 1], {"sp": src}).wait_recv()
+        far = stat_in[0] + stat_in[1]
+        write_log(mine[0:4] + jnp.exp2(-mine[4:8]) * far[0:4], mine[8:12] + jnp.exp2(-mine[12:16]) * far[8:12])
 
     for c in range(0, model, tile):
         cols = slice(c, c + tile)
@@ -614,7 +614,7 @@
         offs_copy(0, 2).wait_send()
         for t in range(2):
             for g in range(groups):
-                kv_copy(t, g).wait_send()
+                kv_copy(0, t, g).wait_send()
             kv_last(t, 0).wait_send()
 
     @pl.when(me == 1)
@@ -629,18 +629,19 @@
 
     @pl.when(me == 2)
     def _():
+        offs_copy(2, 3).wait_send()
         for g in dev1_groups:
             q_copy(2, 1, g).wait_send()
-        for g in range(groups):
-            o_copy(2, 3, g).wait_send()
+            for t in range(2):
+                kv_copy(2, t, g).wait_send()
+        o_copy(2, 3, far_g).wait_send()
         stat_copy(2, 3).wait_send()
 
     @pl.when(me == 3)
     def _():
-        for g in range(groups):
-            if g in dev1_groups:
-                q_copy(3, 1, g).wait_send()
-            q_copy(3, 2, g).wait_send()
+        for g in dev1_groups:
+            q_copy(3, 1, g).wait_send()
+        q_copy(3, 2, far_g).wait_send()
 
 
 def place(mixed, mass_log, out_ref, log_ref, sem):
@@ -691,7 +692,7 @@
             pltpu.VMEM((3, groups, rows, LANES), bf16),
             pltpu.VMEM((2, groups, rows, LANES), bf16),
             pltpu.VMEM((2, groups, rows, LANES), bf16),
-            pltpu.VMEM((2, heads, rows), bf16),
+            pltpu.VMEM((3, heads, rows), bf16),
             pltpu.VMEM((2, groups, rows, LANES), bf16),
             pltpu.VMEM((2, groups, rows, LANES), bf16),
             pltpu.VMEM((2, 16, rows), f32),
@@ -714,8 +715,9 @@
             pltpu.VMEM((slabs, rows, LANES), f32),
             pltpu.VMEM((rows, LANES), f32),
             pltpu.VMEM((rows, LANES), f32),
-            dma((6,)), dma((rows // min(64, rows),)), dma((5, chans // (2 * LANES))), dma((2,)), dma((2, groups)), dma((2, groups)), dma((2, groups)), dma((2, groups)), dma((2,)), dma((2, 2)), dma((2,)), dma((2,)),
+            dma((6,)), dma((rows // min(64, rows),)), dma((5, chans // (2 * LANES))), dma((2,)), dma((2, groups)), dma((2, groups)), dma((2, groups)), dma((2, groups)), dma((2,)), dma((2, 2)), dma((3,)), dma((3,)),
             dma((2, groups)), dma((2, groups)), dma((2,)), dma((2,)), dma((tiles,)), dma((tiles,)), dma, dma, dma, dma,
+            pltpu.SemaphoreType.REGULAR,
         ],
         compiler_params=pltpu.CompilerParams(
             collective_id=0, has_side_effects=True, vmem_limit_bytes=56 * 1024 * 1024),

time: 29.3 us -> 27.2 us (0.928)
  the two profiles are of different devices: /device:TPU:27 before, /device:TPU:23 now
where the time goes in v5:
time: 27.2 us; the launch traced here: 27 us
  Pallas kernels  26.2 us (96%)
  between operations  0.8 us (3%)
    pallas_call x1, Pallas kernels, local(): pl.pallas_call(functools.partial(kernel, n, tp, taps, chans * tp), out_sh...  25.4 us
    pallas_call x1, Pallas kernels, local(): pl.pallas_call(place, out_shape=(jax.ShapeDtypeStruct((share, model), bf1...  0.81 us

profile of v5, /device:TPU:23, one launch (start us, length us, event | category | flops | bytes accessed | tf_op | source)
XLA Modules:
  0.0 27.0 jit_solution(17771742425140843573)
XLA Ops:
  0.6 25.4 %shard_map.149 = (bf16[128,2048]{1,0:T(8,128)(2,1)S(1)}, f32[8,256]{1,0:T(8,128)S(1)}) custom-call(bf16[256,2048]{1,0:T(8,128)(2,1)} %bitcast.8, bf16[2048]{0:T(1024)(128)(2,1)} %ngain_hbm.1, bf16[8,256]{1,0:T(8,128)(2,1)} %bitcast.9, bf16[31,512]{1,0:T(8,128)(2,1)} %taps_hbm.1, bf16[512]{0:T(512)(128)(2,1)} %gain_hbm.1, bf16[512]{0:T(512)(128)(2,1)} %cgain_hbm.1, ...), custom_call_target="tpu_custom_call" | custom-call | tf_op jit(solution)/shard_map/pallas_call | solution.py:676
  26.0 0.8 %shard_map.150 = (bf16[128,2048]{1,0:T(8,128)(2,1)}, f32[8,256]{1,0:T(8,128)}) custom-call(bf16[128,2048]{1,0:T(8,128)(2,1)S(1)} %get-tuple-element.6.mixed, f32[8,256]{1,0:T(8,128)S(1)} %get-tuple-element.7.mass_log), custom_call_target="tpu_custom_call" | custom-call | tf_op jit(solution)/shard_map/pallas_call | solution.py:726

commit v6 on v5

--- a/solution.py
+++ b/solution.py
@@ -25,10 +25,10 @@
     out_ref, log_ref,
     ngain, offs, raw_taps, gain_ref, cgain_ref, cshift_ref,
     stream, normed, weights, out_weights, packet, q_in, kv_in, offs_in, o_out, o_in, stat_out, stat_in,
-    own_r, own_t, far_r, far_t, masses, off_rows, tap_ref, heads_ref, conv_ref, conv_share, leaving, arrived_ref,
+    own_r, own_t, far_r, far_t, masses, off_rows, tap_ref, heads_ref, conv_ref, conv_share, leaving, arrived_ref, heads_last, partner_heads, partner_weights,
     gated, halo, ext, filt, stats, stats_got,
     small_sem, stream_sem, weight_sem, out_weight_sem, q_send, q_recv, kv_send, kv_recv, kv_last_send, kv_last_recv, offs_send, offs_recv,
-    o_send, o_recv, stat_send, stat_recv, out_send, out_recv, halo_send, halo_recv, chan_send, chan_recv, entered,
+    o_send, o_recv, stat_send, stat_recv, out_send, out_recv, halo_send, halo_recv, chan_send, chan_recv, entered, swap_send, swap_recv,
 ):
     f32, bf16 = jnp.float32, jnp.bfloat16
     me = lax.axis_index("sp")
@@ -78,7 +78,14 @@
         (ngain_hbm, ngain), (offs_hbm, offs), (taps_hbm, raw_taps), (gain_hbm, gain_ref),
         (cgain_hbm, cgain_ref), (cshift_hbm, cshift_ref)))]
     gate_copies = [weight_copy(w, 3 + t, half) for half in range(halves) for t, w in enumerate((in_hbm, gate_hbm))]
-    out_copies = [local_copy(w, out_weights.at[t], out_weight_sem.at[t]) for t, w in enumerate((filter_hbm, attend_hbm))]
+    filter_copy = local_copy(filter_hbm, out_weights.at[0], out_weight_sem.at[0])
+    final = groups - 1
+    cut = final * LANES
+
+    def attend_copies(first):
+        early = local_copy(attend_hbm.at[pl.ds(LANES if first else 0, cut)], out_weights.at[1, pl.ds(0, cut)], out_weight_sem.at[1])
+        late = local_copy(attend_hbm.at[pl.ds(0 if first else cut, LANES)], out_weights.at[1, pl.ds(cut, LANES)], out_weight_sem.at[2])
+        return early, late
     for c in range(rows // band):
         stream_copy(c).start()
     small[0].start()
@@ -189,19 +196,25 @@
         def _():
             if half == 0:
                 offs_copy(2, 3).start()
-            q_copy(2, 1, 1 + half).start()
+            if half == 0:
+                q_copy(2, 1, 1).start()
             for g in groups_here:
                 if g in dev1_groups:
                     kv_copy(2, 0, g).start()
 
         @pl.when(me == 3)
         def _():
-            q_copy(3, 1, 1 + half).start()
-            if half == 1:
+            if half == 0:
+                q_copy(3, 1, 1).start()
+            else:
                 q_copy(3, 2, far_g).start()
 
-    for copy in out_copies:
-        copy.start()
+    filter_copy.start()
+    for first, here in ((True, me == 1), (False, me != 1)):
+        @pl.when(here)
+        def _(first=first):
+            for copy in attend_copies(first):
+                copy.start()
     tap_ref[...] = jnp.zeros_like(tap_ref)
     for c in range(slabs):
         tap_ref[c, :taps] = raw_taps[:, c * LANES:(c + 1) * LANES].astype(f32)
@@ -237,8 +250,7 @@
     for d in (2, 3):
         @pl.when(me == d)
         def _(d=d):
-            for g in dev1_groups[2:]:
-                q_copy(d, 1, g).start()
+            q_copy(d, 1, 2).start()
 
     @pl.when(me < n - 1)
     def _():
@@ -318,7 +330,7 @@
     tile = min(1024, model)
 
     def conv_product():
-        out_copies[0].wait()
+        filter_copy.wait()
         for c in range(0, model, tile):
             conv_share[:, c:c + tile] = jnp.dot(
                 conv_ref[...], out_weights[0, :, c:c + tile], preferred_element_type=f32)
@@ -399,6 +411,15 @@
         t = jnp.transpose(masses[which])
         return jnp.concatenate([t[0:8], t[HEAD_DIM:HEAD_DIM + 8]], axis=0)
 
+    blocks = (lax.broadcasted_iota(jnp.int32, (LANES, LANES), 0) // HEAD_DIM
+              == lax.broadcasted_iota(jnp.int32, (LANES, LANES), 1) // HEAD_DIM).astype(bf16)
+
+    def close(place_at, g, o):
+        sq = jnp.dot((o * o).astype(bf16), blocks, preferred_element_type=f32)
+        gain = gain_ref[g * LANES:(g + 1) * LANES].astype(f32).reshape(1, LANES)
+        cols = slice(place_at * LANES, (place_at + 1) * LANES)
+        heads_ref[:, cols] = (o * lax.rsqrt(sq * (1.0 / HEAD_DIM) + rms_eps) * gain).astype(bf16)
+
     @pl.when((me == 0) | (me == 3))
     def _():
         @pl.loop(0, groups // 2)
@@ -406,6 +427,10 @@
             for u in range(2):
                 near_blocks(2 * half + u, [])
 
+            @pl.when((me == 3) & (half == 0))
+            def _():
+                q_copy(3, 1, 3).start()
+
     @pl.when(me == 1)
     def _():
         near_blocks(far_g, [])
@@ -413,8 +438,8 @@
 
         @pl.loop(1, groups)
         def _(g):
-            for i in (1, 0):
-                q_from(i + 2, 1, g).wait_recv()
+            q_from(2, 1, g).wait_recv()
+            q_from(3, 1, g).wait_recv()
             rest = near_blocks(g, [q_in[1, g], q_in[0, g]])
             for h in range(2):
                 for i in (1, 0):
@@ -444,6 +469,7 @@
     @pl.when(me == 2)
     def _():
         near_blocks(1, [])
+        q_copy(2, 1, 3).start()
 
         @pl.loop(1, 2)
         def _(half):
@@ -489,17 +515,13 @@
         stat_out[1] = stat_rows(2)
         stat_copy(2, 3).start()
 
+    @pl.when(me == 1)
+    def _():
+        for g in dev1_groups:
+            close(g - 1, g, pair(own_r[g, 0], own_r[g, 1]))
+
     channel_norm()
     conv_product()
-
-    @pl.when(me == 1)
-    def _():
-        keys, values = kv_from(0, far_g)
-        for h in range(2):
-            res, _ = attend([packet[0, far_g]], keys[h], values[h], off_of(1, far_g, h), False)[0]
-            res = own_r[far_g, h] + own_t[far_g, h] * res
-            own_r[far_g, h] = res
-            note(0, far_g, h, res, res)
 
     @pl.when(me == 3)
     def _():
@@ -515,57 +537,44 @@
                 near = masses[0][:, (HEAD_DIM, 0)[h] + 4 + g:(HEAD_DIM, 0)[h] + 5 + g]
                 note(0, g, h, res, total + near)
 
-    blocks = (lax.broadcasted_iota(jnp.int32, (LANES, LANES), 0) // HEAD_DIM
-              == lax.broadcasted_iota(jnp.int32, (LANES, LANES), 1) // HEAD_DIM).astype(bf16)
-
     def finish(g):
-        cols = slice(g * LANES, (g + 1) * LANES)
-
-        def close(o):
-            sq = jnp.dot((o * o).astype(bf16), blocks, preferred_element_type=f32)
-            gain = gain_ref[cols].astype(f32).reshape(1, LANES)
-            heads_ref[:, cols] = (o * lax.rsqrt(sq * (1.0 / HEAD_DIM) + rms_eps) * gain).astype(bf16)
-
         own = pair(own_r[g, 0], own_r[g, 1])
 
-        @pl.when(me < 2)
+        @pl.when(me == 0)
         def _():
-            close(own)
+            close(g, g, own)
 
         @pl.when(me == 2)
         def _():
             if g == far_g:
-                close(own)
+                close(g, g, own)
             else:
                 through = pair(own_t[g, 0], own_t[g, 1])
                 send(o_out.at[0, g], o_in.at[0, g], o_send.at[0, g], o_recv.at[0, g], {"sp": 1}).wait_recv()
-                close(own + through * o_in[0, g].astype(f32))
+                close(g, g, own + through * o_in[0, g].astype(f32))
 
         @pl.when(me == 3)
         def _():
             through = pair(own_t[g, 0], own_t[g, 1])
             src = 2 if g == far_g else 1
             send(o_out.at[1, g], o_in.at[src - 1, g], o_send.at[1, g], o_recv.at[src - 1, g], {"sp": src}).wait_recv()
-            close(own + through * o_in[src - 1, g].astype(f32))
-
-    out_copies[1].wait()
-    early = groups // 2
-    for g in range(early):
-        finish(g)
-    cut = early * LANES
-    for c in range(0, model, tile):
-        conv_share[:, c:c + tile] += jnp.dot(
-            heads_ref[:, :cut], out_weights[1, :cut, c:c + tile], preferred_element_type=f32)
-    for g in range(early, groups):
-        finish(g)
+            close(g, g, own + through * o_in[src - 1, g].astype(f32))
+
+    for copy in attend_copies(False):
+        copy.wait()
     share = rows // tp
     theirs = pl.ds(pl.multiple_of(partner * share, share), share)
     ours = pl.ds(pl.multiple_of(core * share, share), share)
+    weight_swap = send(out_weights.at[1, pl.ds(cut, LANES)], partner_weights, swap_send.at[0], swap_recv.at[0], {"tp": partner})
+    heads_swap = send(heads_last.at[theirs], partner_heads, swap_send.at[1], swap_recv.at[1], {"tp": partner})
+    weight_swap.start()
+    for g in range(final):
+        finish(g)
     leaves = []
     for c in range(0, model, tile):
         cols = slice(c, c + tile)
         leaving[:, cols] = (conv_share[theirs, cols] + jnp.dot(
-            heads_ref[theirs, cut:], out_weights[1, cut:, cols], preferred_element_type=f32)).astype(bf16)
+            heads_ref[theirs, :cut], out_weights[1, :cut, cols], preferred_element_type=f32)).astype(bf16)
         copy = send(leaving.at[:, pl.ds(c, tile)], arrived_ref.at[:, pl.ds(c, tile)],
                     out_send.at[c // tile], out_recv.at[c // tile], {"tp": partner})
         copy.start()
@@ -573,6 +582,27 @@
     for c in range(0, model, tile):
         cols = slice(c, c + tile)
         conv_share[ours, cols] += jnp.dot(
+            heads_ref[ours, :cut], out_weights[1, :cut, cols], preferred_element_type=f32)
+    @pl.when(me == 1)
+    def _():
+        keys, values = kv_from(0, far_g)
+        parts = []
+        for h in range(2):
+            res, _ = attend([packet[0, far_g]], keys[h], values[h], off_of(1, far_g, h), False)[0]
+            res = own_r[far_g, h] + own_t[far_g, h] * res
+            note(0, far_g, h, res, res)
+            parts.append(res)
+        close(final, far_g, pair(*parts))
+
+    finish(final)
+    heads_last[...] = heads_ref[:, cut:]
+    heads_swap.start()
+    for copy in leaves:
+        copy.wait()
+    weight_swap.wait()
+    for c in range(0, model, tile):
+        cols = slice(c, c + tile)
+        conv_share[ours, cols] += arrived_ref[:, cols].astype(f32) + jnp.dot(
             heads_ref[ours, cut:], out_weights[1, cut:, cols], preferred_element_type=f32)
 
     mine = stat_rows(0)
@@ -599,10 +629,11 @@
         far = stat_in[0] + stat_in[1]
         write_log(mine[0:4] + jnp.exp2(-mine[4:8]) * far[0:4], mine[8:12] + jnp.exp2(-mine[12:16]) * far[8:12])
 
+    heads_swap.wait()
     for c in range(0, model, tile):
         cols = slice(c, c + tile)
-        leaves[c // tile].wait()
-        out_ref[:, cols] = (conv_share[ours, cols] + arrived_ref[:, cols].astype(f32)).astype(bf16)
+        out_ref[:, cols] = (conv_share[ours, cols] + jnp.dot(
+            partner_heads[...], partner_weights[:, cols], preferred_element_type=f32)).astype(bf16)
 
     @pl.when(me < n - 1)
     def _():
@@ -709,15 +740,18 @@
             pltpu.VMEM((rows, model), f32),
             pltpu.VMEM((share, model), bf16),
             pltpu.VMEM((share, model), bf16),
+            pltpu.VMEM((rows, LANES), bf16),
+            pltpu.VMEM((share, LANES), bf16),
+            pltpu.VMEM((LANES, model), bf16),
             pltpu.VMEM((HALO, chans), bf16),
             pltpu.VMEM((HALO, chans), bf16),
             pltpu.VMEM((slabs, HALO + rows, LANES), f32),
             pltpu.VMEM((slabs, rows, LANES), f32),
             pltpu.VMEM((rows, LANES), f32),
             pltpu.VMEM((rows, LANES), f32),
-            dma((6,)), dma((rows // min(64, rows),)), dma((5, chans // (2 * LANES))), dma((2,)), dma((2, groups)), dma((2, groups)), dma((2, groups)), dma((2, groups)), dma((2,)), dma((2, 2)), dma((3,)), dma((3,)),
+            dma((6,)), dma((rows // min(64, rows),)), dma((5, chans // (2 * LANES))), dma((3,)), dma((2, groups)), dma((2, groups)), dma((2, groups)), dma((2, groups)), dma((2,)), dma((2, 2)), dma((3,)), dma((3,)),
             dma((2, groups)), dma((2, groups)), dma((2,)), dma((2,)), dma((tiles,)), dma((tiles,)), dma, dma, dma, dma,
-            pltpu.SemaphoreType.REGULAR,
+            pltpu.SemaphoreType.REGULAR, dma((2,)), dma((2,)),
         ],
         compiler_params=pltpu.CompilerParams(
             collective_id=0, has_side_effects=True, vmem_limit_bytes=56 * 1024 * 1024),

time: 27.2 us -> 26.7 us (0.982)
  the two profiles are of different devices: /device:TPU:23 before, /device:TPU:13 now
where the time goes in v6:
time: 26.7 us; the launch traced here: 26.5 us
  Pallas kernels  25.7 us (96%)
  between operations  0.8 us (3%)
    pallas_call x1, Pallas kernels, local(): pl.pallas_call(functools.partial(kernel, n, tp, taps, chans * tp), out_sh...  24.9 us
    pallas_call x1, Pallas kernels, local(): pl.pallas_call(place, out_shape=(jax.ShapeDtypeStruct((share, model), bf1...  0.81 us

profile of v6, /device:TPU:13, one launch (start us, length us, event | category | flops | bytes accessed | tf_op | source)
XLA Modules:
  0.0 26.5 jit_solution(13349128147109492941)
XLA Ops:
  0.6 24.9 %shard_map.149 = (bf16[128,2048]{1,0:T(8,128)(2,1)S(1)}, f32[8,256]{1,0:T(8,128)S(1)}) custom-call(bf16[256,2048]{1,0:T(8,128)(2,1)} %bitcast.8, bf16[2048]{0:T(1024)(128)(2,1)} %ngain_hbm.1, bf16[8,256]{1,0:T(8,128)(2,1)} %bitcast.9, bf16[31,512]{1,0:T(8,128)(2,1)} %taps_hbm.1, bf16[512]{0:T(512)(128)(2,1)} %gain_hbm.1, bf16[512]{0:T(512)(128)(2,1)} %cgain_hbm.1, ...), custom_call_target="tpu_custom_call" | custom-call | tf_op jit(solution)/shard_map/pallas_call | solution.py:707
  25.6 0.8 %shard_map.150 = (bf16[128,2048]{1,0:T(8,128)(2,1)}, f32[8,256]{1,0:T(8,128)}) custom-call(bf16[128,2048]{1,0:T(8,128)(2,1)S(1)} %get-tuple-element.6.mixed, f32[8,256]{1,0:T(8,128)S(1)} %get-tuple-element.7.mass_log), custom_call_target="tpu_custom_call" | custom-call | tf_op jit(solution)/shard_map/pallas_call | solution.py:760

commit v7 on v6

--- a/solution.py
+++ b/solution.py
@@ -16,6 +16,18 @@
 LANES = 128
 LOG2E = 1.4426950408889634
 MESH = pl.DeviceIdType.MESH
+
+
+class Slots:
+    def __init__(self, pick):
+        self.pick = pick
+
+    @property
+    def at(self):
+        return self
+
+    def __getitem__(self, index):
+        return self.pick(*index) if isinstance(index, tuple) else self.pick(index)
 
 
 def kernel(
@@ -27,10 +39,19 @@
     stream, normed, weights, out_weights, packet, q_in, kv_in, offs_in, o_out, o_in, stat_out, stat_in,
     own_r, own_t, far_r, far_t, masses, off_rows, tap_ref, heads_ref, conv_ref, conv_share, leaving, arrived_ref, heads_last, partner_heads, partner_weights,
     gated, halo, ext, filt, stats, stats_got,
-    small_sem, stream_sem, weight_sem, out_weight_sem, q_send, q_recv, kv_send, kv_recv, kv_last_send, kv_last_recv, offs_send, offs_recv,
-    o_send, o_recv, stat_send, stat_recv, out_send, out_recv, halo_send, halo_recv, chan_send, chan_recv, entered, swap_send, swap_recv,
+    weight_sem, out_weight_sem, flow_send, flow_recv, offs_sem_send, offs_sem_recv,
+    out_send, out_recv, halo_send, halo_recv, chan_send, chan_recv, entered, swap_send, swap_recv,
 ):
     f32, bf16 = jnp.float32, jnp.bfloat16
+    small_sem = Slots(lambda t: (out_weight_sem.at[t] if t < 3 else out_send.at[t - 3] if t < 5 else swap_send.at[0]))
+    stream_sem = Slots(lambda c: flow_send.at[0, c])
+    kv_send, o_send = flow_send, flow_send
+    q_send = Slots(lambda i, g: flow_send.at[2, g])
+    kv_last_send = Slots(lambda t: flow_send.at[2, t])
+    kv_recv, kv_last_recv = flow_recv, flow_recv
+    q_recv = Slots(lambda i, g: flow_recv.at[2 + i, g])
+    o_recv = q_recv
+    stat_recv = Slots(lambda i: flow_recv.at[3, 1 + i])
     me = lax.axis_index("sp")
     core = lax.axis_index("tp")
     partner = 1 - core
@@ -68,7 +89,7 @@
             def _(s=order[t]):
                 weight_copy(projections[s], s, half).start()
 
-    band = min(64, rows)
+    band = rows // packet.shape[1]
 
     def stream_copy(c):
         some = pl.ds(pl.multiple_of(c * band, band), band)
@@ -143,14 +164,16 @@
                     kv_last_send.at[t], kv_last_recv.at[t, src_dev], {"sp": 2})
 
     def offs_copy(src_dev, dst_dev):
-        return send(offs, offs_in.at[src_dev], offs_send.at[dst_dev - 1], offs_recv.at[src_dev], {"sp": dst_dev})
+        return send(offs, offs_in.at[src_dev], offs_sem_send.at[int((src_dev, dst_dev) == (0, 2))], offs_sem_recv.at[src_dev % 2],
+                    {"sp": dst_dev})
 
     def o_copy(src_dev, dst_dev, g):
         return send(o_out.at[dst_dev - 2, g], o_in.at[src_dev - 1, g], o_send.at[dst_dev - 2, g],
                     o_recv.at[src_dev - 1, g], {"sp": dst_dev})
 
     def stat_copy(src_dev, dst_dev):
-        return send(stat_out.at[dst_dev - 2], stat_in.at[src_dev - 1], stat_send.at[dst_dev - 2],
+        return send(stat_out.at[dst_dev - 2], stat_in.at[src_dev - 1],
+                    flow_send.at[2, dst_dev] if src_dev == 1 else flow_send.at[0, 0],
                     stat_recv.at[src_dev - 1], {"sp": dst_dev})
 
     def keep(slot, half, y):
@@ -401,7 +424,7 @@
         return split_keys(kv_in[0, g]), split_values(kv_in[1, g])
 
     def offs_from(src_dev, dst_dev, row):
-        send(offs, offs_in.at[src_dev], offs_send.at[dst_dev - 1], offs_recv.at[src_dev], {"sp": src_dev}).wait_recv()
+        send(offs, offs_in.at[src_dev], offs_sem_send.at[0], offs_sem_recv.at[src_dev % 2], {"sp": src_dev}).wait_recv()
         off_rows[row] = offs_in[src_dev].astype(f32) * LOG2E
 
     def off_of(row, g, h):
@@ -625,7 +648,7 @@
     @pl.when(me == 3)
     def _():
         for src in (1, 2):
-            send(stat_out.at[1], stat_in.at[src - 1], stat_send.at[1], stat_recv.at[src - 1], {"sp": src}).wait_recv()
+            send(stat_out.at[1], stat_in.at[src - 1], flow_send.at[2, 2], stat_recv.at[src - 1], {"sp": src}).wait_recv()
         far = stat_in[0] + stat_in[1]
         write_log(mine[0:4] + jnp.exp2(-mine[4:8]) * far[0:4], mine[8:12] + jnp.exp2(-mine[12:16]) * far[8:12])
 
@@ -749,9 +772,8 @@
             pltpu.VMEM((slabs, rows, LANES), f32),
             pltpu.VMEM((rows, LANES), f32),
             pltpu.VMEM((rows, LANES), f32),
-            dma((6,)), dma((rows // min(64, rows),)), dma((5, chans // (2 * LANES))), dma((3,)), dma((2, groups)), dma((2, groups)), dma((2, groups)), dma((2, groups)), dma((2,)), dma((2, 2)), dma((3,)), dma((3,)),
-            dma((2, groups)), dma((2, groups)), dma((2,)), dma((2,)), dma((tiles,)), dma((tiles,)), dma, dma, dma, dma,
-            pltpu.SemaphoreType.REGULAR, dma((2,)), dma((2,)),
+            dma((5, chans // (2 * LANES))), dma((3,)), dma((3, groups)), dma((4, groups)), dma((2,)), dma((2,)),
+            dma((tiles,)), dma((tiles,)), dma, dma, dma, dma, pltpu.SemaphoreType.REGULAR, dma((2,)), dma((2,)),
         ],
         compiler_params=pltpu.CompilerParams(
             collective_id=0, has_side_effects=True, vmem_limit_bytes=56 * 1024 * 1024),

time: 26.7 us -> 26.4 us (0.989)
  the two profiles are of different devices: /device:TPU:13 before, /device:TPU:15 now
where the time goes in v7:
time: 26.4 us; the launch traced here: 26.3 us
  Pallas kernels  25.5 us (97%)
  between operations  0.8 us (3%)
    pallas_call x1, Pallas kernels, local(): pl.pallas_call(functools.partial(kernel, n, tp, taps, chans * tp), out_sh...  24.6 us
    pallas_call x1, Pallas kernels, local(): pl.pallas_call(place, out_shape=(jax.ShapeDtypeStruct((share, model), bf1...  0.81 us

profile of v7, /device:TPU:15, one launch (start us, length us, event | category | flops | bytes accessed | tf_op | source)
XLA Modules:
  0.0 26.3 jit_solution(1280585659220341081)
XLA Ops:
  0.6 24.6 %shard_map.149 = (bf16[128,2048]{1,0:T(8,128)(2,1)S(1)}, f32[8,256]{1,0:T(8,128)S(1)}) custom-call(bf16[256,2048]{1,0:T(8,128)(2,1)} %bitcast.8, bf16[2048]{0:T(1024)(128)(2,1)} %ngain_hbm.1, bf16[8,256]{1,0:T(8,128)(2,1)} %bitcast.9, bf16[31,512]{1,0:T(8,128)(2,1)} %taps_hbm.1, bf16[512]{0:T(512)(128)(2,1)} %gain_hbm.1, bf16[512]{0:T(512)(128)(2,1)} %cgain_hbm.1, ...), custom_call_target="tpu_custom_call" | custom-call | tf_op jit(solution)/shard_map/pallas_call | solution.py:730
  25.3 0.8 %shard_map.150 = (bf16[128,2048]{1,0:T(8,128)(2,1)}, f32[8,256]{1,0:T(8,128)}) custom-call(bf16[128,2048]{1,0:T(8,128)(2,1)S(1)} %get-tuple-element.6.mixed, f32[8,256]{1,0:T(8,128)S(1)} %get-tuple-element.7.mass_log), custom_call_target="tpu_custom_call" | custom-call | tf_op jit(solution)/shard_map/pallas_call | solution.py:782

commit v8 on v7

--- a/solution.py
+++ b/solution.py
@@ -360,7 +360,7 @@
 
     ri = lax.broadcasted_iota(jnp.int32, (rows, rows), 0)
     ci = lax.broadcasted_iota(jnp.int32, (rows, rows), 1)
-    tri = (ri >= ci).astype(bf16)
+    tri = (ri > ci).astype(bf16)
 
     def split_keys(k):
         zero = jnp.zeros_like(k)
@@ -383,13 +383,15 @@
             head = jnp.where(strict, x[:rows], 0.0)
             return jnp.concatenate([head, x[rows:]], axis=0) if len(blocks_q) > 1 else head
 
-        cum = jnp.dot(masked(lose).astype(bf16), tri, preferred_element_type=f32)
-        w = masked(jnp.exp2(z - cum))
+        gain = z - lose
+        lose = masked(lose)
+        beyond = jnp.dot(lose.astype(bf16), tri, preferred_element_type=f32)
+        w = masked(jnp.exp2(gain - beyond))
         res = jnp.dot(w.astype(bf16), v, preferred_element_type=f32)
         pieces = []
         for r in range(len(blocks_q)):
             some = slice(r * rows, (r + 1) * rows)
-            pieces.append((res[some], jnp.broadcast_to(cum[some, 0:1], (rows, LANES))))
+            pieces.append((res[some], jnp.broadcast_to(beyond[some, 0:1] + lose[some, 0:1], (rows, LANES))))
         return pieces
 
     def note(which, g, h, res, total):

time: 26.4 us -> 26.5 us (level)
  no operation moved by 1% of the time
where the time goes in v8:
time: 26.5 us; the launch traced here: 26.3 us
  Pallas kernels  25.5 us (96%)
  between operations  0.8 us (3%)
    pallas_call x1, Pallas kernels, local(): pl.pallas_call(functools.partial(kernel, n, tp, taps, chans * tp), out_sh...  24.7 us
    pallas_call x1, Pallas kernels, local(): pl.pallas_call(place, out_shape=(jax.ShapeDtypeStruct((share, model), bf1...  0.81 us

profile of v8, /device:TPU:15, one launch (start us, length us, event | category | flops | bytes accessed | tf_op | source)
XLA Modules:
  0.0 26.3 jit_solution(14324367530568091621)
XLA Ops:
  0.6 24.7 %shard_map.149 = (bf16[128,2048]{1,0:T(8,128)(2,1)S(1)}, f32[8,256]{1,0:T(8,128)S(1)}) custom-call(bf16[256,2048]{1,0:T(8,128)(2,1)} %bitcast.8, bf16[2048]{0:T(1024)(128)(2,1)} %ngain_hbm.1, bf16[8,256]{1,0:T(8,128)(2,1)} %bitcast.9, bf16[31,512]{1,0:T(8,128)(2,1)} %taps_hbm.1, bf16[512]{0:T(512)(128)(2,1)} %gain_hbm.1, bf16[512]{0:T(512)(128)(2,1)} %cgain_hbm.1, ...), custom_call_target="tpu_custom_call" | custom-call | tf_op jit(solution)/shard_map/pallas_call | solution.py:732
  25.3 0.8 %shard_map.150 = (bf16[128,2048]{1,0:T(8,128)(2,1)}, f32[8,256]{1,0:T(8,128)}) custom-call(bf16[128,2048]{1,0:T(8,128)(2,1)S(1)} %get-tuple-element.6.mixed, f32[8,256]{1,0:T(8,128)S(1)} %get-tuple-element.7.mass_log), custom_call_target="tpu_custom_call" | custom-call | tf_op jit(solution)/shard_map/pallas_call | solution.py:784
